TPU v7x, 32 devices: a whole 2x2x4 slice. The times are simulated.
32 devices in a mesh: sp: 8 (over z, core), tp: 4 (over y, x).
Axes of the slice: x: 2, y: 2, z: 4, core: 2. Of those that a mesh axis runs over, the one named last changes fastest.
Arguments:
- skip_path_vectors: bfloat16 [2048, 2048], P('sp'), may hold values from -10 to 10
- asker_raw_scores: bfloat16 [2048, 2048], P('sp', 'tp'), may hold values from -6 to 6
- retain_raw_scores: bfloat16 [2048, 2048], P('sp', 'tp'), may hold values from -5.5 to 5.5
- memory_write_entries: bfloat16 [2048, 2048], P('sp', 'tp'), may hold values from -6 to 6
- emit_switch_scores: bfloat16 [2048, 2048], P('sp', 'tp'), may hold values from -6 to 6
- retain_minimum_share: float32 [2048], P('tp'), may hold values from 0.88 to 0.99990234
- extra_shrink_rate: float32 [16, 2048], P('tp', 'sp'), may hold values from -0.7 to 0
- lane_rescale_factor: float32 [128], replicated, may hold values from 0.1 to 1.9
- emit_projection_array: bfloat16 [2048, 2048], P('tp'), may hold values from -0.1875 to 0.1875
- specialist_rescale_factor: float32 [2048], replicated, may hold values from 0.1 to 1.9
- specialist_switch_proj: bfloat16 [8, 2048, 4096], P('sp', None, 'tp'), may hold values from -0.125 to 0.125
- specialist_raise_proj: bfloat16 [8, 2048, 4096], P('sp', None, 'tp'), may hold values from -0.125 to 0.125
- specialist_lower_proj: bfloat16 [8, 4096, 2048], P('sp', 'tp'), may hold values from -0.375 to 0.375
- specialist_choice_ids: int32 [2048, 2], P('sp'), may hold values from 0 to 7, all different within a row; in each aligned block of 256 rows (0 to 255, 256 to 511, ...) at most 96 rows name the same one
- cluster_chance: float32 [2048], P('sp'), may hold values from 0.1 to 0.6
- specialist_duo_scores: float32 [2048, 2], P('sp'), may hold values from -2 to 2
Outputs:
- mixed_out: bfloat16 [2048, 2048], P('sp', 'tp')
Inputs may be any that keep to these rules, and one draw needn't show every extreme that they name: `specialist_choice_ids`: in each aligned block of 256 rows (the rows of one index of sp) no expert is named by more than 96 rows, a bound that some block reaches; the 2 ids of a row differ.
All inputs are finite; a program needn't handle non-finite values.
Results may differ from a plain program's by a relative error of at most 0.02.
Values may be sent and summed in bfloat16 or wider, within the bound.
A program may use at most 64 MiB of HBM per device.

v0:
```python
import functools

import jax
import jax.numpy as jnp
from jax import lax
from jax.experimental import pallas as pl
from jax.experimental.pallas import tpu as pltpu
from jax.sharding import PartitionSpec as P

EPS = 1e-06
PRECISE = lax.Precision.HIGHEST


MESH = pl.DeviceIdType.MESH
VMEM = pl.BlockSpec(memory_space=pltpu.VMEM)
VMEM_LIMIT = 60 * 1024 * 1024


def each(first, last, body):
    if last - first <= 8:
        for i in range(first, last):
            body(i)
    else:

        @pl.loop(first, last)
        def _(i):
            body(i)


def push(src, dst, send_sem, recv_sem, peer):
    return pltpu.make_async_remote_copy(
        src_ref=src,
        dst_ref=dst,
        send_sem=send_sem,
        recv_sem=recv_sem,
        device_id=peer,
        device_id_type=MESH,
    )


def state_kernel(sp_size, own_ref, out_ref, far_send, far_recv, near_send, near_recv):
    me = lax.axis_index("sp")
    pairs = sp_size // 2
    partner = me + 1 - 2 * lax.rem(me, 2)
    barrier = pltpu.get_barrier_semaphore()
    pl.semaphore_signal(barrier, inc=1, device_id={"sp": partner}, device_id_type=MESH)

    def far(d):
        return lax.rem(me + 2 * d, sp_size)

    def source(d):
        return lax.rem(me + sp_size - 2 * d, sp_size)

    def far_copy(d):
        return push(own_ref, out_ref.at[me], far_send.at[d], far_recv.at[d], {"sp": far(d)})

    def near_copy(d):
        block = own_ref if d is None else out_ref.at[source(d)]
        place = me if d is None else source(d)
        slot = 0 if d is None else d
        return push(
            block, out_ref.at[place], near_send.at[slot], near_recv.at[slot], {"sp": partner}
        )

    each(
        1,
        pairs,
        lambda d: pl.semaphore_signal(
            barrier, inc=1, device_id={"sp": far(d)}, device_id_type=MESH
        ),
    )
    pl.semaphore_wait(barrier, pairs)
    each(1, pairs, lambda d: far_copy(d).start())
    near_copy(None).start()

    def relay(d):
        far_copy(d).wait_recv()
        near_copy(d).start()

    each(1, pairs, relay)
    out_ref[me] = own_ref[...]
    near_copy(None).wait()

    def finish(d):
        far_copy(d).wait_send()
        near_copy(d).wait()

    each(1, pairs, finish)


def gather_states(packed):
    sp_size = lax.axis_size("sp")
    pairs = sp_size // 2
    dma = pltpu.SemaphoreType.DMA((pairs,))
    return pl.pallas_call(
        functools.partial(state_kernel, sp_size),
        out_shape=jax.ShapeDtypeStruct((sp_size,) + packed.shape, packed.dtype),
        in_specs=[VMEM],
        out_specs=VMEM,
        scratch_shapes=[dma, dma, dma, dma],
        compiler_params=pltpu.CompilerParams(collective_id=0, has_side_effects=True),
    )(packed)


def expert_kernel(
    sp_size,
    tp_size,
    group,
    mixer_ref,
    proj_ref,
    skip_ref,
    gain_ref,
    places_ref,
    gate_hbm,
    up_hbm,
    down_hbm,
    ret_ref,
    resid_ref,
    gate_w,
    up_w,
    down_w,
    pj,
    pj_in,
    sq,
    slots_in,
    slots,
    arr,
    part,
    got,
    hid,
    total,
    load_sem,
    pj_send,
    pj_recv,
    sq_send,
    sq_recv,
    out_send,
    out_recv,
    ag_send,
    ag_recv,
    rs_send,
    rs_recv,
    back_send,
    back_recv,
):
    my_s = lax.axis_index("sp")
    my_t = lax.axis_index("tp")
    tokens, width = skip_ref.shape
    cap = slots.shape[1]
    hidden_width = gate_w.shape[1]
    model_width = gate_w.shape[0]
    groups = sp_size // group
    rows = group * cap

    loads = [
        pltpu.make_async_copy(src, dst, load_sem.at[i])
        for i, (src, dst) in enumerate(((gate_hbm, gate_w), (up_hbm, up_w), (down_hbm, down_w)))
    ]
    barrier = pltpu.get_barrier_semaphore()

    def tp_of(j):
        return lax.rem(my_t + j, tp_size)

    def tp_from(j):
        return lax.rem(my_t + tp_size - j, tp_size)

    def sp_of(k):
        return lax.rem(my_s + k, sp_size)

    def sp_from(k):
        return lax.rem(my_s + sp_size - k, sp_size)

    each(
        1,
        tp_size,
        lambda j: pl.semaphore_signal(barrier, inc=1, device_id={"tp": tp_of(j)}, device_id_type=MESH),
    )
    each(
        1,
        sp_size,
        lambda k: pl.semaphore_signal(barrier, inc=1, device_id={"sp": sp_of(k)}, device_id_type=MESH),
    )
    for load in loads:
        load.start()

    def project(t):
        cols = pl.ds(pl.multiple_of(t * width, width), width)
        return jnp.dot(mixer_ref[...], proj_ref[:, cols], preferred_element_type=jnp.float32).astype(
            jnp.bfloat16
        )

    def pj_copy(j):
        return push(pj.at[j], pj_in.at[j], pj_send.at[j], pj_recv.at[j], {"tp": tp_of(j)})

    def project_all(j):
        pj[j] = project(tp_of(j))

    each(1, tp_size, project_all)
    pl.semaphore_wait(barrier, tp_size + sp_size - 2)
    each(1, tp_size, lambda j: pj_copy(j).start())
    total[...] = project(my_t).astype(jnp.float32)

    def add_in(j):
        pj_copy(j).wait_recv()
        total[...] += pj_in[j].astype(jnp.float32)

    each(1, tp_size, add_in)
    resid = (skip_ref[...].astype(jnp.float32) + total[...]).astype(jnp.bfloat16)
    resid_ref[...] = resid
    wide = resid.astype(jnp.float32)
    row_sums = jnp.sum(wide * wide, axis=1, keepdims=True)
    sq[0] = jnp.transpose(jnp.broadcast_to(row_sums, (tokens, 128)))[:8]

    def sq_copy(j):
        return push(sq.at[0], sq.at[j], sq_send.at[j], sq_recv.at[j], {"tp": tp_of(j)})

    each(1, tp_size, lambda j: sq_copy(j).start())
    slot_ids = lax.broadcasted_iota(jnp.int32, (sp_size * cap, tokens), 0)
    chosen = (slot_ids == places_ref[0:1, :]) | (slot_ids == places_ref[1:2, :])
    one_hot = chosen.astype(jnp.float32).astype(jnp.bfloat16)
    each(1, tp_size, lambda j: sq_copy(j).wait())
    squares = jnp.sum(sq[...], axis=0)[0:1]
    squares = jnp.transpose(jnp.broadcast_to(squares, (128, tokens)))[:, 0:1]
    normed = (wide * lax.rsqrt(squares / model_width + EPS) * gain_ref[...]).astype(jnp.bfloat16)
    filled = jnp.dot(one_hot, normed, preferred_element_type=jnp.float32).astype(jnp.bfloat16)
    slots_in[...] = filled.reshape(sp_size, cap, width)
    arr[my_t, 0] = filled[:cap]

    def out_copy(k):
        return push(
            slots_in.at[k], arr.at[my_t, k], out_send.at[k], out_recv.at[k], {"sp": sp_of(k)}
        )

    each(1, sp_size, lambda k: out_copy(k).start())

    def span(g):
        return pl.ds(g * group, group)

    def ag_copy(g, j):
        block = arr.at[my_t, span(g)]
        return push(block, block, ag_send.at[j, g], ag_recv.at[j, g], {"tp": tp_of(j)})

    def rs_copy(g, j):
        return push(
            part.at[j, span(g)],
            got.at[j, span(g)],
            rs_send.at[j, g],
            rs_recv.at[j, g],
            {"tp": tp_of(j)},
        )

    def back_copy(k):
        return push(
            slots.at[k], ret_ref.at[k], back_send.at[k], back_recv.at[k], {"sp": sp_from(k)}
        )


    def dispatch(g):
        def take(i):
            out_copy(g * group + i).wait_recv()

        each(1 if isinstance(g, int) and g == 0 else 0, group, take)
        each(1, tp_size, lambda j: ag_copy(g, j).start())

    dispatch(0)
    each(1, groups, dispatch)
    for load in loads:
        load.wait()
    tile = min(256, hidden_width)

    @pl.loop(0, groups)
    def _(g):
        each(1, tp_size, lambda j: ag_copy(g, j).wait_recv())

        @pl.loop(0, hidden_width // tile)
        def _(f):
            cols = pl.ds(pl.multiple_of(f * tile, tile), tile)
            gate = jnp.zeros((rows, tile), jnp.float32)
            up = jnp.zeros((rows, tile), jnp.float32)
            for t in range(tp_size):
                x = arr[t, span(g)].reshape(rows, width)
                depth = slice(t * width, (t + 1) * width)
                gate += jnp.dot(x, gate_w[depth, cols], preferred_element_type=jnp.float32)
                up += jnp.dot(x, up_w[depth, cols], preferred_element_type=jnp.float32)
            hid[:, cols] = (gate * jax.nn.sigmoid(gate) * up).astype(jnp.bfloat16)

        def lower(j):
            cols = pl.ds(pl.multiple_of(tp_of(j) * width, width), width)
            out = jnp.dot(hid[...], down_w[:, cols], preferred_element_type=jnp.float32)
            part[j, span(g)] = out.astype(jnp.bfloat16).reshape(group, cap, width)

        each(1, tp_size, lower)
        each(1, tp_size, lambda j: rs_copy(g, j).start())
        lower(0)

    def give_back(g):
        acc = part[0, span(g)].astype(jnp.float32)
        for j in range(1, tp_size):
            rs_copy(g, j).wait_recv()
            acc += got[j, span(g)].astype(jnp.float32)
        slots[span(g)] = acc.astype(jnp.bfloat16)
        each(
            1 if isinstance(g, int) and g == 0 else 0,
            group,
            lambda i: back_copy(g * group + i).start(),
        )

    give_back(0)
    each(1, groups, give_back)
    ret_ref[0] = slots[0]
    each(1, sp_size, lambda k: back_copy(k).wait())
    each(1, sp_size, lambda k: out_copy(k).wait_send())

    def drain(j):
        pj_copy(j).wait_send()
        for g in range(groups):
            ag_copy(g, j).wait_send()
            rs_copy(g, j).wait_send()

    each(1, tp_size, drain)


def run_experts(mixer_out, projection, skip_cols, gain_cols, places, gate, up, down, cap):
    sp_size = lax.axis_size("sp")
    tp_size = lax.axis_size("tp")
    tokens, width = skip_cols.shape
    model_width, hidden_width = gate.shape
    group = max(g for g in range(1, sp_size + 1) if sp_size % g == 0 and g * cap <= 256)
    groups = sp_size // group
    bf, f32 = jnp.bfloat16, jnp.float32
    dma = pltpu.SemaphoreType.DMA
    anywhere = pl.BlockSpec(memory_space=pl.ANY)
    return pl.pallas_call(
        functools.partial(expert_kernel, sp_size, tp_size, group),
        out_shape=(
            jax.ShapeDtypeStruct((sp_size, cap, width), bf),
            jax.ShapeDtypeStruct((tokens, width), bf),
        ),
        in_specs=[VMEM] * 5 + [anywhere] * 3,
        out_specs=(VMEM, VMEM),
        scratch_shapes=[
            pltpu.VMEM((model_width, hidden_width), bf),
            pltpu.VMEM((model_width, hidden_width), bf),
            pltpu.VMEM((hidden_width, model_width), bf),
            pltpu.VMEM((tp_size, tokens, width), bf),
            pltpu.VMEM((tp_size, tokens, width), bf),
            pltpu.VMEM((tp_size, 8, tokens), f32),
            pltpu.VMEM((sp_size, cap, width), bf),
            pltpu.VMEM((sp_size, cap, width), bf),
            pltpu.VMEM((tp_size, sp_size, cap, width), bf),
            pltpu.VMEM((tp_size, sp_size, cap, width), bf),
            pltpu.VMEM((tp_size, sp_size, cap, width), bf),
            pltpu.VMEM((group * cap, hidden_width), bf),
            pltpu.VMEM((tokens, width), f32),
            dma((3,)),
            dma((tp_size,)),
            dma((tp_size,)),
            dma((tp_size,)),
            dma((tp_size,)),
            dma((sp_size,)),
            dma((sp_size,)),
            dma((tp_size, groups)),
            dma((tp_size, groups)),
            dma((tp_size, groups)),
            dma((tp_size, groups)),
            dma((sp_size,)),
            dma((sp_size,)),
        ],
        compiler_params=pltpu.CompilerParams(
            collective_id=1, has_side_effects=True, vmem_limit_bytes=VMEM_LIMIT
        ),
    )(mixer_out, projection, skip_cols, gain_cols, places, gate, up, down)


def carry_states(totals, own_state):
    lanes, depth = totals.shape
    sp_size = lax.axis_size("sp")
    place = lax.axis_index("sp")
    pad = -lanes % 16
    packed = jnp.concatenate(
        [
            own_state.astype(jnp.bfloat16).reshape(lanes * depth, depth),
            totals.astype(jnp.bfloat16),
            jnp.zeros((pad, depth), jnp.bfloat16),
        ]
    )
    gathered = gather_states(packed)
    states = gathered[:, : lanes * depth].reshape(sp_size, lanes, depth, depth)
    shrinks = gathered[:, lanes * depth : lanes * depth + lanes].astype(jnp.float32)
    factor = jnp.ones((lanes, depth), jnp.float32)
    carried = jnp.zeros((lanes, depth, depth), jnp.float32)
    for lap in reversed(range(sp_size)):
        earlier = lap < place
        held = states[lap].astype(jnp.float32) * factor[:, :, None]
        carried = carried + jnp.where(earlier, held, 0.0)
        factor = jnp.where(earlier, factor * shrinks[lap], factor)
    return carried


def shards(
    skip_path_vectors,
    asker_raw_scores,
    retain_raw_scores,
    memory_write_entries,
    emit_switch_scores,
    retain_minimum_share,
    extra_shrink_rate,
    lane_rescale_factor,
    emit_projection_array,
    specialist_rescale_factor,
    specialist_switch_proj,
    specialist_raise_proj,
    specialist_lower_proj,
    specialist_choice_ids,
    cluster_chance,
    specialist_duo_scores,
):
    token_count_total = skip_path_vectors.shape[0]
    model_width = skip_path_vectors.shape[1]
    head_depth = lane_rescale_factor.shape[0]
    lanes_on_device = extra_shrink_rate.shape[0]
    retain_share = retain_minimum_share + (1.0 - retain_minimum_share) * jax.nn.sigmoid(
        retain_raw_scores.astype(jnp.float32)
    )
    retain_share = retain_share.reshape(token_count_total, lanes_on_device, head_depth)
    shrink_log_rate = jnp.log(retain_share) + extra_shrink_rate.T[:, :, None]
    key_rows = 1.0 - retain_share
    queries = jax.nn.silu(asker_raw_scores.astype(jnp.float32)).reshape(
        token_count_total, lanes_on_device, head_depth
    )
    values = memory_write_entries.astype(jnp.float32).reshape(
        token_count_total, lanes_on_device, head_depth
    )
    cumulative = jnp.cumsum(shrink_log_rate, axis=0)
    query_tilde = queries * jnp.exp(cumulative)
    key_tilde = key_rows * jnp.exp(-cumulative)
    causal = jnp.arange(token_count_total)[:, None] >= jnp.arange(token_count_total)[None, :]
    scores = jnp.einsum("thd,shd->hts", query_tilde, key_tilde, precision=PRECISE)
    scores = jnp.where(causal[None], scores, 0.0)
    inside = jnp.einsum("hts,shv->thv", scores, values, precision=PRECISE)
    totals = jnp.exp(cumulative[-1])
    own_state = jnp.einsum("shd,shv->hdv", key_tilde * totals[None], values, precision=PRECISE)
    carried = carry_states(totals, own_state)
    outside = jnp.einsum("thd,hdv->thv", query_tilde, carried, precision=PRECISE)
    readout = inside + outside
    normed_heads = readout * lax.rsqrt(jnp.mean(readout * readout, axis=-1, keepdims=True) + EPS)
    gated_out = (
        normed_heads
        * lane_rescale_factor
        * jax.nn.silu(
            emit_switch_scores.astype(jnp.float32).reshape(
                token_count_total, lanes_on_device, head_depth
            )
        )
    )
    mixer_out = gated_out.reshape(token_count_total, lanes_on_device * head_depth).astype(
        jnp.bfloat16
    )
    tp_size = lax.axis_size("tp")
    sp_size = lax.axis_size("sp")
    experts = sp_size
    top_count = specialist_choice_ids.shape[1]
    capacity = -(-3 * token_count_total * top_count // (2 * experts))
    capacity = -(-capacity // 16) * 16
    flat_ids = specialist_choice_ids.reshape(-1)
    matches = (flat_ids[:, None] == jnp.arange(experts, dtype=jnp.int32)[None, :]).astype(jnp.int32)
    before = jnp.cumsum(matches, axis=0) - matches
    turn = lax.rem(flat_ids + sp_size - lax.axis_index("sp"), sp_size)
    places = turn * capacity + jnp.sum(before * matches, axis=1)
    places = places.reshape(token_count_total, top_count)
    col_width = model_width // tp_size
    col_start = lax.axis_index("tp") * col_width
    skip_cols = lax.dynamic_slice_in_dim(skip_path_vectors, col_start, col_width, 1)
    gain_cols = lax.dynamic_slice_in_dim(specialist_rescale_factor, col_start, col_width, 0)
    returned, resid_cols = run_experts(
        mixer_out,
        emit_projection_array,
        skip_cols,
        gain_cols[None, :],
        places.T,
        specialist_switch_proj[0],
        specialist_raise_proj[0],
        specialist_lower_proj[0],
        capacity,
    )
    returned = returned.reshape(sp_size * capacity, col_width)
    slot_ids = jnp.arange(sp_size * capacity, dtype=jnp.int32)[None, :]
    picked = jnp.stack(
        [
            jnp.dot(
                (places[:, j : j + 1] == slot_ids).astype(jnp.bfloat16),
                returned,
                preferred_element_type=jnp.float32,
            )
            for j in range(top_count)
        ],
        axis=1,
    )
    spread_logit = specialist_duo_scores[:, 0] - specialist_duo_scores[:, 1]
    weights = cluster_chance[:, None] * jnp.stack(
        [jax.nn.sigmoid(spread_logit), jax.nn.sigmoid(-spread_logit)], axis=1
    )
    mixed_out = resid_cols.astype(jnp.float32) + jnp.sum(
        weights[:, :, None] * picked.astype(jnp.float32), axis=1
    )
    return mixed_out.astype(jnp.bfloat16)


def solution(mesh):
    return jax.shard_map(
        shards,
        mesh=mesh,
        in_specs=(
            P("sp", None),
            P("sp", "tp"),
            P("sp", "tp"),
            P("sp", "tp"),
            P("sp", "tp"),
            P("tp"),
            P("tp", "sp"),
            P(),
            P("tp", None),
            P(),
            P("sp", None, "tp"),
            P("sp", None, "tp"),
            P("sp", "tp", None),
            P("sp", None),
            P("sp"),
            P("sp", None),
        ),
        out_specs=P("sp", "tp"),
        check_vma=False,
    )
```

profile of v0, /device:TPU:1, one launch (start us, length us, event | category | flops | bytes accessed | tf_op | source)
XLA Modules:
  0.0 150.4 jit_solution(14481069306177626628)
XLA Ops:
  0.0 1.2 copy.54
  1.9 0.9 broadcast_subtract_fusion
  2.8 0.7 add_bitcast_fusion
  5.2 1.2 broadcast_multiply_fusion
  7.1 0.8 maximum_maximum_fusion.own_ref
  7.9 18.3 %shard_map.154 = bf16[8,528,128]{2,1,0:T(8,128)(2,1)} custom-call(bf16[528,128]{1,0:T(8,128)(2,1)} %maximum_maximum_fusion.own_ref), custom_call_target="tpu_custom_call" | custom-call | tf_op jit(solution)/shard_map/pallas_call | solution.py:95
  26.3 0.7 slice_convert_fusion
  27.6 0.9 convert_select_fusion
  28.7 2.0 %fusion.66 = (bf16[1,512,128]{2,1,0:T(8,128)(2,1)S(1)}, bf16[1,512,128]{2,1,0:T(8,128)(2,1)S(1)}, bf16[1,512,128]{2,1,0:T(8,128)(2,1)}, bf16[1,512,128]{2,1,0:T(...) fusion(bf16[8,528,128]{2,1,0:T(8,128)(2,1)} %shard_map.154), kind=kLoop, calls=%fused_computation.118 | loop fusion | bytes 1835008 | tf_op jit(solution)/shard_map/slice | solution.py:394
  31.0 0.8 copy.68
  31.8 0.8 copy.69
  32.6 1.8 %copy.70 = f32[4,128,128]{1,2,0:T(8,128)} copy(bf16[4,128,128]{2,1,0:T(8,128)(2,1)} %bitcast.131) | data formatting | bytes 393216 | tf_op jit(solution)/shard_map/convert_element_type | solution.py:394
  34.4 0.8 copy.71
  35.2 2.0 %convolution_bitcast_fusion = f32[256,4,128]{0,2,1:T(8,128)S(1)} fusion(f32[256,4,128]{2,1,0:T(4,128)S(1)} %get-tuple-element.27, f32[4,128,128]{1,2,0:T(8,128)} %copy.71, f32[4,128,128]{1,2,0:T(8,128)} %copy.70, f32[4,128,128]{1,2,0:T(8,128)} %copy.69, f32[4,128,128]{1,2,0:T(8,128)} %copy.68, f32[4,128,128]{1,2,0:T(8,128)S(1)} %copy.67, ...), kind=kOutput, calls=%fused_computation.1 | convolution fusion | flops 202702848 | bytes 3160071 | tf_op jit(solution)/shard_map/thd,hdv->thv/dot_general | solution.py:444
  37.3 1.0 convolution_select_fusion
  38.3 0.7 multiply_reduce_fusion
  39.6 0.8 copy.80.mixer_ref
  40.7 1.3 reduce-window.16
  43.4 0.7 constant_dynamic-slice_fusion.skip_ref
  44.1 1.3 dynamic_slice.7
  45.5 100.7 %shard_map.155 = (bf16[8,96,512]{2,1,0:T(8,128)(2,1)}, bf16[256,512]{1,0:T(8,128)(2,1)}) custom-call(bf16[256,512]{1,0:T(8,128)(2,1)} %copy.80.mixer_ref, bf16[512,2048]{1,0:T(8,128)(2,1)} %proj_ref.1, bf16[256,512]{1,0:T(8,128)(2,1)} %constant_dynamic-slice_fusion.skip_ref, f32[1,512]{1,0:T(1,128)} %bitcast.140, s32[2,256]{1,0:T(2,128)} %bitcast.138, ...), custom_call_target="tpu_custom_call" | custom-call | tf_op jit(solution)/shard_map/pallas_call | solution.py:333
  146.3 1.6 %convolution_bitcast_fusion.3 = f32[256,1,512]{2,0,1:T(8,128)S(1)} fusion(bf16[768,512]{1,0:T(8,128)(2,1)} %bitcast.118, s32[256]{0:T(256)S(1)} %bitcast.143), kind=kOutput, calls=%fused_computation.5 | convolution fusion | flops 201523200 | bytes 1311744 | tf_op jit(solution)/shard_map/dot_general | solution.py:490
  147.9 1.5 %convolution_bitcast_fusion.2 = f32[256,1,512]{2,0,1:T(8,128)S(1)} fusion(bf16[768,512]{1,0:T(8,128)(2,1)} %bitcast.119, s32[256]{0:T(256)S(1)} %bitcast.142), kind=kOutput, calls=%fused_computation.4 | convolution fusion | flops 201523200 | bytes 1311744 | tf_op jit(solution)/shard_map/dot_general | solution.py:490
  149.6 0.8 add_convert_fusion
  (63 shorter events, 6.4 us)
Async XLA Ops:
  0.0 43.4 %copy-start = (bf16[256,2048]{1,0:T(8,128)(2,1)S(1)}, bf16[256,2048]{1,0:T(8,128)(2,1)}, u32[]{:S(2)}) copy-start(bf16[256,2048]{1,0:T(8,128)(2,1)} %param.16) | copy-start | bytes 3145732
  3.7 1.0 copy-start.4
  4.9 1.5 copy-start.2
  32.6 4.6 %copy-start.1 = (f32[256,4,128]{2,1,0:T(4,128)S(1)}, f32[256,4,128]{2,1,0:T(4,128)}, u32[]{:S(2)}) copy-start(f32[256,4,128]{2,1,0:T(4,128)} %get-tuple-element.19) | copy-start | bytes 1572868
  38.3 1.0 copy-start.3
  38.3 1.1 copy-start.10
  38.3 2.1 %copy-start.7 = (s32[256,2]{0,1:T(2,128)S(1)}, s32[256,2]{0,1:T(2,128)}, u32[]{:S(2)}) copy-start(s32[256,2]{0,1:T(2,128)} %param.29) | copy-start | bytes 6148
  45.5 100.8 %copy-start.6 = (s32[256,2]{0,1:T(2,128)S(1)}, s32[256,2]{0,1:T(2,128)}, u32[]{:S(2)}) copy-start(s32[256,2]{0,1:T(2,128)} %fusion.58) | copy-start | bytes 6148
  146.2 3.2 %copy-start.8 = (f32[256,2]{0,1:T(2,128)S(1)}, f32[256,2]{0,1:T(2,128)}, u32[]{:S(2)}) copy-start(f32[256,2]{0,1:T(2,128)} %param.31) | copy-start | bytes 6148
  146.2 3.2 %copy-start.9 = (f32[256]{0:T(256)S(1)}, f32[256]{0:T(256)}, u32[]{:S(2)}) copy-start(f32[256]{0:T(256)} %param.30) | copy-start | bytes 3076
  146.3 3.4 %copy-start.5 = (bf16[256,512]{1,0:T(8,128)(2,1)S(1)}, bf16[256,512]{1,0:T(8,128)(2,1)}, u32[]{:S(2)}) copy-start(bf16[256,512]{1,0:T(8,128)(2,1)} %get-tuple-element.7) | copy-start | bytes 786436
where the time goes:
time: 153 us; the launch traced here: 150 us
  Pallas kernels  119 us (78%)
  local copies, waits for them, and re-layouts  13 us (8%)
  other arithmetic  10.4 us (7%)
  matrix products  7.53 us (5%)
    pallas_call x1, Pallas kernels, run_experts(): pl.pallas_call(functools.partial(expert_kernel, sp_size, tp_size, group),...  101 us
    pallas_call x1, Pallas kernels, gather_states(): pl.pallas_call(functools.partial(state_kernel, sp_size), out_shape=jax.Sh...  18.3 us
    convert_element_type x7, local copies, waits for them, and re-layouts, carry_states(): held = states[lap].astype(jnp.float32) * factor[:, :, None]  4.54 us
    dot_general x2, matrix products, shards(): jnp.dot((places[:, j:j + 1] == slot_ids).astype(jnp.bfloat16), returned,...  3.12 us

commit v1 on v0

v1 whole, which is shorter than its diff:
```python
import functools

import jax
import jax.numpy as jnp
from jax import lax
from jax.experimental import pallas as pl
from jax.experimental.pallas import tpu as pltpu
from jax.sharding import PartitionSpec as P

EPS = 1e-06
PRECISE = lax.Precision.HIGHEST


MESH = pl.DeviceIdType.MESH
VMEM = pl.BlockSpec(memory_space=pltpu.VMEM)
VMEM_LIMIT = 60 * 1024 * 1024


def each(first, last, body):
    if last - first <= 8:
        for i in range(first, last):
            body(i)
    else:

        @pl.loop(first, last)
        def _(i):
            body(i)


def push(src, dst, send_sem, recv_sem, peer):
    return pltpu.make_async_remote_copy(
        src_ref=src,
        dst_ref=dst,
        send_sem=send_sem,
        recv_sem=recv_sem,
        device_id=peer,
        device_id_type=MESH,
    )


def state_kernel(sp_size, own_ref, out_ref, far_send, far_recv, near_send, near_recv):
    me = lax.axis_index("sp")
    pairs = sp_size // 2
    partner = me + 1 - 2 * lax.rem(me, 2)
    barrier = pltpu.get_barrier_semaphore()
    pl.semaphore_signal(barrier, inc=1, device_id={"sp": partner}, device_id_type=MESH)

    def far(d):
        return lax.rem(me + 2 * d, sp_size)

    def source(d):
        return lax.rem(me + sp_size - 2 * d, sp_size)

    def far_copy(d):
        return push(own_ref, out_ref.at[me], far_send.at[d], far_recv.at[d], {"sp": far(d)})

    def near_copy(d):
        block = own_ref if d is None else out_ref.at[source(d)]
        place = me if d is None else source(d)
        slot = 0 if d is None else d
        return push(
            block, out_ref.at[place], near_send.at[slot], near_recv.at[slot], {"sp": partner}
        )

    each(
        1,
        pairs,
        lambda d: pl.semaphore_signal(
            barrier, inc=1, device_id={"sp": far(d)}, device_id_type=MESH
        ),
    )
    pl.semaphore_wait(barrier, pairs)
    each(1, pairs, lambda d: far_copy(d).start())
    near_copy(None).start()

    def relay(d):
        far_copy(d).wait_recv()
        near_copy(d).start()

    each(1, pairs, relay)
    out_ref[me] = own_ref[...]
    near_copy(None).wait()

    def finish(d):
        far_copy(d).wait_send()
        near_copy(d).wait()

    each(1, pairs, finish)


def gather_states(packed):
    sp_size = lax.axis_size("sp")
    pairs = sp_size // 2
    dma = pltpu.SemaphoreType.DMA((pairs,))
    return pl.pallas_call(
        functools.partial(state_kernel, sp_size),
        out_shape=jax.ShapeDtypeStruct((sp_size,) + packed.shape, packed.dtype),
        in_specs=[VMEM],
        out_specs=VMEM,
        scratch_shapes=[dma, dma, dma, dma],
        compiler_params=pltpu.CompilerParams(collective_id=0, has_side_effects=True),
    )(packed)


def grid_of(tp_size):
    cols = max(d for d in range(1, tp_size + 1) if tp_size % d == 0 and d * d <= tp_size)
    return tp_size // cols, cols


def flip(index, mask):
    bit = 1
    while bit <= mask:
        if mask & bit:
            index = index + bit * (1 - 2 * lax.rem(index // bit, 2))
        bit *= 2
    return index


def partner_order(sp_size):
    unit = max(1, sp_size // 8)
    blocks = [list(range(i * unit, (i + 1) * unit)) for i in range(sp_size // unit)]
    if len(blocks) > 2:
        blocks = [blocks[0]] + blocks[2:] + [blocks[1]]
    return unit, [mask for block in blocks for mask in block]


class Scatter:
    def __init__(self, grid, part, got, comb, got2, s1, r1, s2, r2):
        self.grid = grid
        self.part, self.got, self.comb, self.got2 = part, got, comb, got2
        self.s1, self.r1, self.s2, self.r2 = s1, r1, s2, r2

    def sizes(self, u):
        rows, cols = self.grid.shape
        return (cols, rows) if u % 2 == 0 else (rows, cols)

    def place(self, u, i, j):
        n1, n2 = self.sizes(u)
        return i * n2 + j if u % 2 == 0 else j * n2 + i

    def first(self, u, a):
        n1, n2 = self.sizes(u)
        peer = self.grid.along_row(a) if u % 2 == 0 else self.grid.along_col(a)
        span = pl.ds(a * n2, n2)
        return push(
            self.part.at[u, span], self.got.at[u, span], self.s1.at[u, a], self.r1.at[u, a], {"tp": peer}
        )

    def second(self, u, b):
        peer = self.grid.along_col(b) if u % 2 == 0 else self.grid.along_row(b)
        return push(self.comb.at[u, b], self.got2.at[u, b], self.s2.at[u, b], self.r2.at[u, b], {"tp": peer})

    def start(self, u):
        for a in range(1, self.sizes(u)[0]):
            self.first(u, a).start()

    def middle(self, u):
        n1, n2 = self.sizes(u)
        for a in range(1, n1):
            self.first(u, a).wait_recv()
        for b in range(1, n2):
            self.comb[u, b] = self.near_sum(u, b).astype(jnp.bfloat16)
            self.second(u, b).start()

    def near_sum(self, u, b):
        n1, n2 = self.sizes(u)
        acc = self.part[u, b].astype(jnp.float32)
        for a in range(1, n1):
            acc += self.got[u, a * n2 + b].astype(jnp.float32)
        return acc

    def finish(self, u):
        acc = self.near_sum(u, 0)
        for b in range(1, self.sizes(u)[1]):
            self.second(u, b).wait_recv()
            acc += self.got2[u, b].astype(jnp.float32)
        return acc

    def drain(self, u):
        n1, n2 = self.sizes(u)
        for a in range(1, n1):
            self.first(u, a).wait_send()
        for b in range(1, n2):
            self.second(u, b).wait_send()


class Grid:
    def __init__(self, tp_size):
        self.shape = grid_of(tp_size)
        me = lax.axis_index("tp")
        self.row, self.col = me // self.shape[1], lax.rem(me, self.shape[1])

    def at(self, i, j):
        rows, cols = self.shape
        return lax.rem(self.row + j, rows) * cols + lax.rem(self.col + i, cols)

    def along_row(self, i):
        return self.at(i, 0)

    def along_col(self, j):
        return self.at(0, j)

    def from_row(self, i):
        return self.at(self.shape[1] - i, 0)

    def from_col(self, j):
        return self.at(0, self.shape[0] - j)


def expert_kernel(
    sp_size,
    tp_size,
    cap,
    mixer_ref,
    tok_ref,
    gain_ref,
    skip_hbm,
    proj_hbm,
    gate_hbm,
    up_hbm,
    down_hbm,
    out_ref,
    gate_w,
    up_w,
    down_w,
    proj_w,
    skip_v,
    pj_part,
    pj_got,
    pj_comb,
    pj_got2,
    resid_v,
    sq,
    oh0,
    oh1,
    slots_in,
    arr,
    part,
    got,
    comb,
    got2,
    hid,
    slots,
    ret,
    load_sem,
    pj_s1,
    pj_r1,
    pj_s2,
    pj_r2,
    sq_send,
    sq_recv,
    out_send,
    out_recv,
    own_row_send,
    own_row_recv,
    own_col_send,
    own_col_recv,
    relay_send,
    relay_recv,
    rs_s1,
    rs_r1,
    rs_s2,
    rs_r2,
    back_send,
    back_recv,
):
    my_s = lax.axis_index("sp")
    my_t = lax.axis_index("tp")
    grid = Grid(tp_size)
    grid_rows, grid_cols = grid.shape
    unit, masks = partner_order(sp_size)
    units = sp_size // unit
    unit_rows = unit * cap
    tokens, width = out_ref.shape
    model_width, hidden_width = gate_w.shape
    bf, f32 = jnp.bfloat16, jnp.float32
    half = tokens // 2

    my_cols = pl.ds(pl.multiple_of(my_t * width, width), width)
    pairs_in = (
        (proj_hbm, proj_w),
        (skip_hbm.at[:, my_cols], skip_v),
        (gate_hbm, gate_w),
        (up_hbm, up_w),
        (down_hbm, down_w),
    )
    loads = [pltpu.make_async_copy(src, dst, load_sem.at[i]) for i, (src, dst) in enumerate(pairs_in)]
    barrier = pltpu.get_barrier_semaphore()

    def tp_of(j):
        return lax.rem(my_t + j, tp_size)

    def sp_of(q):
        return flip(my_s, masks[q])

    each(
        1,
        tp_size,
        lambda j: pl.semaphore_signal(barrier, inc=1, device_id={"tp": tp_of(j)}, device_id_type=MESH),
    )
    for q in range(1, sp_size):
        pl.semaphore_signal(barrier, inc=1, device_id={"sp": sp_of(q)}, device_id_type=MESH)
    for load in loads:
        load.start()
    loads[0].wait()
    pl.semaphore_wait(barrier, tp_size + sp_size - 2)

    pj = Scatter(grid, pj_part, pj_got, pj_comb, pj_got2, pj_s1, pj_r1, pj_s2, pj_r2)

    def project(i, j):
        cols = pl.ds(pl.multiple_of(grid.at(i, j) * width, width), width)
        out = jnp.dot(mixer_ref[...], proj_w[:, cols], preferred_element_type=f32).astype(bf)
        pj_part[0, pj.place(0, i, j)] = out[:half]
        pj_part[1, pj.place(1, i, j)] = out[half:]

    targets = [(i, j) for i in range(grid_cols) for j in range(grid_rows)]
    for i, j in targets:
        if i > 0:
            project(i, j)
    pj.start(0)
    for i, j in targets:
        if i == 0 and j > 0:
            project(i, j)
    pj.start(1)
    project(0, 0)

    tok = tok_ref[...]
    lanes = -(-sp_size // 128) * 128
    lane = lax.broadcasted_iota(jnp.int32, (1, lanes), 1)
    base = jnp.zeros((1, lanes), f32)
    for q in range(sp_size):
        base = base + jnp.where(lane == sp_of(q), float(q * cap), 0.0)
    wide_lane = lax.broadcasted_iota(jnp.int32, (tokens, lanes), 1).astype(f32)
    mine = [(wide_lane == tok[:, j : j + 1]).astype(f32) for j in range(2)]
    row_id = lax.broadcasted_iota(jnp.int32, (tokens, tokens), 0)
    col_id = lax.broadcasted_iota(jnp.int32, (tokens, tokens), 1)
    before = (col_id < row_id).astype(f32).astype(bf)
    rank = jnp.dot(before, (mine[0] + mine[1]).astype(bf), preferred_element_type=f32) + base
    slot_ids = lax.broadcasted_iota(jnp.int32, (tokens, sp_size * cap), 1).astype(f32)
    for j, oh in enumerate((oh0, oh1)):
        spot = jnp.sum(rank * mine[j], axis=1, keepdims=True)
        oh[...] = (slot_ids == spot).astype(f32).astype(bf)
    weights = [
        tok[:, 2:3] * jax.nn.sigmoid(tok[:, 3:4] - tok[:, 4:5]),
        tok[:, 2:3] * jax.nn.sigmoid(tok[:, 4:5] - tok[:, 3:4]),
    ]

    pj.middle(0)
    pj.middle(1)
    loads[1].wait()
    total = jnp.concatenate([pj.finish(0), pj.finish(1)], axis=0)
    resid = (skip_v[...].astype(f32) + total).astype(bf)
    resid_v[...] = resid
    wide = resid.astype(f32)
    row_sums = jnp.sum(wide * wide, axis=1, keepdims=True)
    sq[0] = jnp.transpose(jnp.broadcast_to(row_sums, (tokens, 128)))[:8]

    def sq_copy(j):
        return push(sq.at[0], sq.at[j], sq_send.at[j], sq_recv.at[j], {"tp": tp_of(j)})

    each(1, tp_size, lambda j: sq_copy(j).start())
    scaled = wide * gain_ref[:, my_cols]
    each(1, tp_size, lambda j: sq_copy(j).wait())
    squares = jnp.sum(sq[...], axis=0)[0:1]
    squares = jnp.transpose(jnp.broadcast_to(squares, (128, tokens)))[:, 0:1]
    normed = (scaled * lax.rsqrt(squares / model_width + EPS)).astype(bf)

    both = oh0[...] + oh1[...]
    filled = lax.dot_general(
        both, normed, (((0,), (0,)), ((), ())), preferred_element_type=f32
    ).astype(bf)
    slots_in[...] = filled.reshape(sp_size, cap, width)
    arr[my_t, 0, pl.ds(0, cap)] = filled[:cap]

    def out_copy(q):
        dst = arr.at[my_t, q // unit, pl.ds((q % unit) * cap, cap)]
        return push(slots_in.at[q], dst, out_send.at[q], out_recv.at[q], {"sp": sp_of(q)})

    for q in range(1, sp_size):
        out_copy(q).start()

    def own_row(p, i):
        block = arr.at[my_t, p]
        return push(block, block, own_row_send.at[p, i], own_row_recv.at[p, i], {"tp": grid.along_row(i)})

    def own_col(p, j):
        block = arr.at[my_t, p]
        return push(block, block, own_col_send.at[p, j], own_col_recv.at[p, j], {"tp": grid.along_col(j)})

    def relay(p, i, j):
        if p % 2 == 0:
            block, peer = arr.at[grid.from_row(i), p], grid.along_col(j)
        else:
            block, peer = arr.at[grid.from_col(j), p], grid.along_row(i)
        return push(block, block, relay_send.at[p, i, j], relay_recv.at[p, i, j], {"tp": peer})

    def take(p):
        for i in range(unit):
            q = p * unit + i
            if q > 0:
                out_copy(q).wait_recv()
        for i in range(1, grid_cols):
            own_row(p, i).start()
        for j in range(1, grid_rows):
            own_col(p, j).start()

    def pass_on(p):
        if p % 2 == 0:
            for i in range(1, grid_cols):
                own_row(p, i).wait_recv()
                for j in range(1, grid_rows):
                    relay(p, i, j).start()
        else:
            for j in range(1, grid_rows):
                own_col(p, j).wait_recv()
                for i in range(1, grid_cols):
                    relay(p, i, j).start()

    def gathered(p):
        if p % 2 == 0:
            for j in range(1, grid_rows):
                own_col(p, j).wait_recv()
        else:
            for i in range(1, grid_cols):
                own_row(p, i).wait_recv()
        for i in range(1, grid_cols):
            for j in range(1, grid_rows):
                relay(p, i, j).wait_recv()

    rs = Scatter(grid, part, got, comb, got2, rs_s1, rs_r1, rs_s2, rs_r2)
    tile = min(256, hidden_width)

    def compute(g):
        pair = pl.ds(2 * g, 2)

        @pl.loop(0, hidden_width // tile)
        def _(f):
            cols = pl.ds(pl.multiple_of(f * tile, tile), tile)
            gate = jnp.zeros((2 * unit_rows, tile), f32)
            up = jnp.zeros((2 * unit_rows, tile), f32)
            for t in range(tp_size):
                x = arr[t, pair].reshape(2 * unit_rows, width)
                depth = slice(t * width, (t + 1) * width)
                gate += jnp.dot(x, gate_w[depth, cols], preferred_element_type=f32)
                up += jnp.dot(x, up_w[depth, cols], preferred_element_type=f32)
            hid[:, cols] = (gate * jax.nn.sigmoid(gate) * up).astype(bf)

        def lower(i, j):
            cols = pl.ds(pl.multiple_of(grid.at(i, j) * width, width), width)
            out = jnp.dot(hid[...], down_w[:, cols], preferred_element_type=f32).astype(bf)
            part[2 * g, rs.place(2 * g, i, j)] = out[:unit_rows]
            part[2 * g + 1, rs.place(2 * g + 1, i, j)] = out[unit_rows:]

        for i in range(1, grid_cols):
            for j in range(grid_rows):
                lower(i, j)
        rs.start(2 * g)
        for j in range(1, grid_rows):
            lower(0, j)
        rs.start(2 * g + 1)
        lower(0, 0)

    def back_copy(q):
        return push(slots.at[q], ret.at[q], back_send.at[q], back_recv.at[q], {"sp": sp_of(q)})

    def give_back(p):
        done = rs.finish(p).astype(bf)
        for i in range(unit):
            q = p * unit + i
            if q == 0:
                ret[0] = done[:cap]
            else:
                slots[q] = done[i * cap : (i + 1) * cap]
                back_copy(q).start()

    groups = units // 2
    take(0)
    take(1)
    pass_on(0)
    pass_on(1)
    for g in range(groups):
        now = (2 * g, 2 * g + 1)
        if g + 1 < groups:
            take(2 * g + 2)
            take(2 * g + 3)
        if g == 0:
            for load in loads[2:]:
                load.wait()
        for p in now:
            gathered(p)
        compute(g)
        if g + 1 < groups:
            pass_on(2 * g + 2)
            pass_on(2 * g + 3)
        if g >= 1:
            rs.middle(2 * g - 2)
            rs.middle(2 * g - 1)
        if g >= 2:
            give_back(2 * g - 4)
            give_back(2 * g - 3)
    last = units - 2
    rs.middle(last)
    rs.middle(last + 1)
    for p in range(max(0, units - 4), units):
        give_back(p)

    for q in range(1, sp_size):
        back_copy(q).wait_recv()
    returned = ret[...].reshape(sp_size * cap, width)
    mixed = resid_v[...].astype(f32)
    for j, oh in enumerate((oh0, oh1)):
        mixed += weights[j] * jnp.dot(oh[...], returned, preferred_element_type=f32)
    out_ref[...] = mixed.astype(bf)

    for u in range(2):
        pj.drain(u)
    for p in range(units):
        for i in range(1, grid_cols):
            own_row(p, i).wait_send()
            for j in range(1, grid_rows):
                relay(p, i, j).wait_send()
        for j in range(1, grid_rows):
            own_col(p, j).wait_send()
        rs.drain(p)
    for q in range(1, sp_size):
        out_copy(q).wait_send()
        back_copy(q).wait_send()


def run_experts(mixer_out, tok, gain, skip, projection, gate, up, down, cap):
    sp_size = lax.axis_size("sp")
    tp_size = lax.axis_size("tp")
    grid_rows, grid_cols = grid_of(tp_size)
    side = max(grid_rows, grid_cols)
    tokens, model_width = skip.shape
    width = model_width // tp_size
    hidden_width = gate.shape[1]
    unit, masks = partner_order(sp_size)
    units = sp_size // unit
    rows = unit * cap
    half = tokens // 2
    bf, f32 = jnp.bfloat16, jnp.float32
    dma = pltpu.SemaphoreType.DMA
    anywhere = pl.BlockSpec(memory_space=pl.ANY)
    vmem = pltpu.VMEM
    return pl.pallas_call(
        functools.partial(expert_kernel, sp_size, tp_size, cap),
        out_shape=jax.ShapeDtypeStruct((tokens, width), bf),
        in_specs=[VMEM] * 3 + [anywhere] * 5,
        out_specs=VMEM,
        scratch_shapes=[
            vmem(gate.shape, bf),
            vmem(up.shape, bf),
            vmem(down.shape, bf),
            vmem(projection.shape, bf),
            vmem((tokens, width), bf),
            vmem((2, tp_size, half, width), bf),
            vmem((2, tp_size, half, width), bf),
            vmem((2, side, half, width), bf),
            vmem((2, side, half, width), bf),
            vmem((tokens, width), bf),
            vmem((tp_size, 8, tokens), f32),
            vmem((tokens, sp_size * cap), bf),
            vmem((tokens, sp_size * cap), bf),
            vmem((sp_size, cap, width), bf),
            vmem((tp_size, units, rows, width), bf),
            vmem((units, tp_size, rows, width), bf),
            vmem((units, tp_size, rows, width), bf),
            vmem((units, side, rows, width), bf),
            vmem((units, side, rows, width), bf),
            vmem((2 * rows, hidden_width), bf),
            vmem((sp_size, cap, width), bf),
            vmem((sp_size, cap, width), bf),
            dma((5,)),
            dma((2, side)),
            dma((2, side)),
            dma((2, side)),
            dma((2, side)),
            dma((tp_size,)),
            dma((tp_size,)),
            dma((sp_size,)),
            dma((sp_size,)),
            dma((units, grid_cols)),
            dma((units, grid_cols)),
            dma((units, grid_rows)),
            dma((units, grid_rows)),
            dma((units, grid_cols, grid_rows)),
            dma((units, grid_cols, grid_rows)),
            dma((units, side)),
            dma((units, side)),
            dma((units, side)),
            dma((units, side)),
            dma((sp_size,)),
            dma((sp_size,)),
        ],
        compiler_params=pltpu.CompilerParams(
            collective_id=1, has_side_effects=True, vmem_limit_bytes=VMEM_LIMIT
        ),
    )(mixer_out, tok, gain, skip, projection, gate, up, down)


def carry_states(totals, own_state):
    lanes, depth = totals.shape
    sp_size = lax.axis_size("sp")
    place = lax.axis_index("sp")
    pad = -lanes % 16
    packed = jnp.concatenate(
        [
            own_state.astype(jnp.bfloat16).reshape(lanes * depth, depth),
            totals.astype(jnp.bfloat16),
            jnp.zeros((pad, depth), jnp.bfloat16),
        ]
    )
    gathered = gather_states(packed)
    states = gathered[:, : lanes * depth].reshape(sp_size, lanes, depth, depth)
    shrinks = gathered[:, lanes * depth : lanes * depth + lanes].astype(jnp.float32)
    factor = jnp.ones((lanes, depth), jnp.float32)
    carried = jnp.zeros((lanes, depth, depth), jnp.float32)
    for lap in reversed(range(sp_size)):
        earlier = lap < place
        held = states[lap].astype(jnp.float32) * factor[:, :, None]
        carried = carried + jnp.where(earlier, held, 0.0)
        factor = jnp.where(earlier, factor * shrinks[lap], factor)
    return carried


def shards(
    skip_path_vectors,
    asker_raw_scores,
    retain_raw_scores,
    memory_write_entries,
    emit_switch_scores,
    retain_minimum_share,
    extra_shrink_rate,
    lane_rescale_factor,
    emit_projection_array,
    specialist_rescale_factor,
    specialist_switch_proj,
    specialist_raise_proj,
    specialist_lower_proj,
    specialist_choice_ids,
    cluster_chance,
    specialist_duo_scores,
):
    token_count_total = skip_path_vectors.shape[0]
    model_width = skip_path_vectors.shape[1]
    head_depth = lane_rescale_factor.shape[0]
    lanes_on_device = extra_shrink_rate.shape[0]
    retain_share = retain_minimum_share + (1.0 - retain_minimum_share) * jax.nn.sigmoid(
        retain_raw_scores.astype(jnp.float32)
    )
    retain_share = retain_share.reshape(token_count_total, lanes_on_device, head_depth)
    shrink_log_rate = jnp.log(retain_share) + extra_shrink_rate.T[:, :, None]
    key_rows = 1.0 - retain_share
    queries = jax.nn.silu(asker_raw_scores.astype(jnp.float32)).reshape(
        token_count_total, lanes_on_device, head_depth
    )
    values = memory_write_entries.astype(jnp.float32).reshape(
        token_count_total, lanes_on_device, head_depth
    )
    cumulative = jnp.cumsum(shrink_log_rate, axis=0)
    query_tilde = queries * jnp.exp(cumulative)
    key_tilde = key_rows * jnp.exp(-cumulative)
    causal = jnp.arange(token_count_total)[:, None] >= jnp.arange(token_count_total)[None, :]
    scores = jnp.einsum("thd,shd->hts", query_tilde, key_tilde, precision=PRECISE)
    scores = jnp.where(causal[None], scores, 0.0)
    inside = jnp.einsum("hts,shv->thv", scores, values, precision=PRECISE)
    totals = jnp.exp(cumulative[-1])
    own_state = jnp.einsum("shd,shv->hdv", key_tilde * totals[None], values, precision=PRECISE)
    carried = carry_states(totals, own_state)
    outside = jnp.einsum("thd,hdv->thv", query_tilde, carried, precision=PRECISE)
    readout = inside + outside
    normed_heads = readout * lax.rsqrt(jnp.mean(readout * readout, axis=-1, keepdims=True) + EPS)
    gated_out = (
        normed_heads
        * lane_rescale_factor
        * jax.nn.silu(
            emit_switch_scores.astype(jnp.float32).reshape(
                token_count_total, lanes_on_device, head_depth
            )
        )
    )
    mixer_out = gated_out.reshape(token_count_total, lanes_on_device * head_depth).astype(
        jnp.bfloat16
    )
    tp_size = lax.axis_size("tp")
    sp_size = lax.axis_size("sp")
    experts = sp_size
    top_count = specialist_choice_ids.shape[1]
    capacity = -(-3 * token_count_total * top_count // (2 * experts))
    capacity = -(-capacity // 16) * 16
    tok = jnp.concatenate(
        [specialist_choice_ids.astype(jnp.float32), cluster_chance[:, None], specialist_duo_scores], axis=1
    )
    return run_experts(
        mixer_out,
        tok,
        specialist_rescale_factor[None, :],
        skip_path_vectors,
        emit_projection_array,
        specialist_switch_proj[0],
        specialist_raise_proj[0],
        specialist_lower_proj[0],
        capacity,
    )


def solution(mesh):
    return jax.shard_map(
        shards,
        mesh=mesh,
        in_specs=(
            P("sp", None),
            P("sp", "tp"),
            P("sp", "tp"),
            P("sp", "tp"),
            P("sp", "tp"),
            P("tp"),
            P("tp", "sp"),
            P(),
            P("tp", None),
            P(),
            P("sp", None, "tp"),
            P("sp", None, "tp"),
            P("sp", "tp", None),
            P("sp", None),
            P("sp"),
            P("sp", None),
        ),
        out_specs=P("sp", "tp"),
        check_vma=False,
    )
```

time: 153 us -> 128 us (0.84)
  Pallas kernels: 119 us -> 108 us
  local copies, waits for them, and re-layouts: 13 us -> 7.87 us
  other arithmetic: 10.4 us -> 6.62 us
  matrix products: 7.53 us -> 3.91 us
    pallas_call x1, Pallas kernels: 101 us -> 89.5 us  [run_experts(): pl.pallas_call(functools.partial(expert_kernel, sp_size, tp_size, cap), o...]
    convert_element_type x7, local copies, waits for them, and re-layouts: 4.54 us -> 0.79 us  [carry_states(): held = states[lap].astype(jnp.float32) * factor[:, :, None]]
    dot_general x2 -> x0, matrix products: 3.12 us -> none  [shards(): jnp.dot((places[:, j:j + 1] == slot_ids).astype(jnp.bfloat16), returned,...]
    dynamic_slice x2 -> x0, local copies, waits for them, and re-layouts: 2.08 us -> none  [the longest x1 1.34 us: shards(): lax.dynamic_slice_in_dim(specialist_rescale_factor, col_start, col_width, 0)]
where the time goes in v1:
time: 128 us; the launch traced here: 127 us
  Pallas kernels  108 us (84%)
  local copies, waits for them, and re-layouts  7.87 us (6%)
  other arithmetic  6.62 us (5%)
  matrix products  3.91 us (3%)
    pallas_call x1, Pallas kernels, run_experts(): pl.pallas_call(functools.partial(expert_kernel, sp_size, tp_size, cap), o...  89.5 us
    pallas_call x1, Pallas kernels, gather_states(): pl.pallas_call(functools.partial(state_kernel, sp_size), out_shape=jax.Sh...  18.3 us
    unnamed x17, local copies, waits for them, and re-layouts  3 us

profile of v1, /device:TPU:1, one launch (start us, length us, event | category | flops | bytes accessed | tf_op | source)
XLA Modules:
  0.0 126.6 jit_solution(10858750595835498855)
XLA Ops:
  0.0 1.1 copy.82
  1.1 0.7 broadcast_subtract_fusion.1
  1.8 0.9 broadcast_subtract_fusion
  2.7 0.7 add_bitcast_fusion
  3.5 0.2 copy.83
  3.7 0.4 fusion.6
  4.3 0.2 copy.105
  4.9 0.2 copy.104
  5.1 0.4 broadcast_multiply_fusion
  5.5 0.7 convolution_convert_fusion
  6.3 0.8 maximum_maximum_fusion.own_ref
  7.1 18.3 %shard_map.154 = bf16[8,528,128]{2,1,0:T(8,128)(2,1)} custom-call(bf16[528,128]{1,0:T(8,128)(2,1)} %maximum_maximum_fusion.own_ref), custom_call_target="tpu_custom_call" | custom-call | tf_op jit(solution)/shard_map/pallas_call | solution.py:95
  25.5 0.7 slice_convert_fusion
  26.2 0.6 multiply_select_fusion
  26.8 0.9 convert_select_fusion
  27.8 1.3 %fusion.57 = (bf16[1,512,128]{2,1,0:T(8,128)(2,1)S(1)}, bf16[1,512,128]{2,1,0:T(8,128)(2,1)S(1)}, bf16[1,512,128]{2,1,0:T(8,128)(2,1)S(1)}, bf16[1,512,128]{2,1,...) fusion(bf16[8,528,128]{2,1,0:T(8,128)(2,1)} %shard_map.154), kind=kLoop, calls=%fused_computation.93 | loop fusion | bytes 1835008 | tf_op jit(solution)/shard_map/slice | solution.py:621
  30.0 1.5 %convolution_bitcast_fusion = f32[256,4,128]{0,2,1:T(8,128)S(1)} fusion(f32[256,4,128]{2,1,0:T(4,128)S(1)} %get-tuple-element.21, f32[4,128,128]{1,2,0:T(8,128)S(1)} %copy.99, f32[4,128,128]{1,2,0:T(8,128)S(1)} %copy.98, f32[4,128,128]{1,2,0:T(8,128)S(1)} %copy.97, f32[4,128,128]{1,2,0:T(8,128)S(1)} %copy.96, f32[4,128,128]{1,2,0:T(8,128)S(1)} %copy.95, ...), kind=kOutput, calls=%fused_computation.1 | convolution fusion | flops 202702848 | bytes 3160071 | tf_op jit(solution)/shard_map/thd,hdv->thv/dot_general | solution.py:671
  31.5 1.0 convolution_select_fusion
  32.6 0.7 multiply_reduce_fusion
  33.5 0.2 multiply_convert_fusion
  33.7 0.8 copy.106.mixer_ref
  34.6 0.8 copy.103.tok_ref
  35.4 89.5 %shard_map.155 = bf16[256,512]{1,0:T(8,128)(2,1)} custom-call(bf16[256,512]{1,0:T(8,128)(2,1)} %copy.106.mixer_ref, f32[256,5]{1,0:T(8,128)} %copy.103.tok_ref, f32[1,2048]{1,0:T(1,128)} %bitcast.120, bf16[256,2048]{1,0:T(8,128)(2,1)} %skip_hbm.1, bf16[512,2048]{1,0:T(8,128)(2,1)} %proj_hbm.1, bf16[2048,1024]{1,0:T(8,128)(2,1)} %bitcast.98, ...), custom_call_target="tpu_custom_call" | custom-call | tf_op jit(solution)/shard_map/pallas_call | solution.py:546
  124.9 1.7 %copy.129 = bf16[256,512]{1,0:T(8,128)(2,1)} copy(bf16[256,512]{1,0:T(8,128)(2,1)} %shard_map.155) | data formatting | bytes 524288
  (37 shorter events, 1.8 us)
Async XLA Ops:
  0.0 5.5 %copy-start = (bf16[256,512]{1,0:T(8,128)(2,1)S(1)}, bf16[256,512]{1,0:T(8,128)(2,1)}, u32[]{:S(2)}) copy-start(bf16[256,512]{1,0:T(8,128)(2,1)} %param.19) | copy-start | bytes 786436
  3.6 1.0 copy-start.2
  31.5 1.8 %copy-start.1 = (bf16[256,512]{1,0:T(8,128)(2,1)S(1)}, bf16[256,512]{1,0:T(8,128)(2,1)}, u32[]{:S(2)}) copy-start(bf16[256,512]{1,0:T(8,128)(2,1)} %param.20) | copy-start | bytes 786436
  32.6 1.0 copy-start.6
  32.6 2.0 %copy-start.3 = (s32[256,2]{0,1:T(2,128)S(1)}, s32[256,2]{0,1:T(2,128)}, u32[]{:S(2)}) copy-start(s32[256,2]{0,1:T(2,128)} %param.29) | copy-start | bytes 6148
  32.6 2.0 %copy-start.4 = (f32[256,2]{0,1:T(2,128)S(1)}, f32[256,2]{0,1:T(2,128)}, u32[]{:S(2)}) copy-start(f32[256,2]{0,1:T(2,128)} %param.31) | copy-start | bytes 6148
  32.6 2.0 %copy-start.5 = (f32[256]{0:T(256)S(1)}, f32[256]{0:T(256)}, u32[]{:S(2)}) copy-start(f32[256]{0:T(256)} %param.30) | copy-start | bytes 3076

commit v2 on v1

v2 whole, which is shorter than its diff:
```python
import functools

import jax
import jax.numpy as jnp
from jax import lax
from jax.experimental import pallas as pl
from jax.experimental.pallas import tpu as pltpu
from jax.sharding import PartitionSpec as P

EPS = 1e-06
MESH = pl.DeviceIdType.MESH
VMEM = pl.BlockSpec(memory_space=pltpu.VMEM)
VMEM_LIMIT = 56 * 1024 * 1024


def each(first, last, body):
    if last - first <= 8:
        for i in range(first, last):
            body(i)
    else:

        @pl.loop(first, last)
        def _(i):
            body(i)


def push(src, dst, send_sem, recv_sem, peer):
    return pltpu.make_async_remote_copy(
        src_ref=src,
        dst_ref=dst,
        send_sem=send_sem,
        recv_sem=recv_sem,
        device_id=peer,
        device_id_type=MESH,
    )


def grid_of(tp_size):
    cols = max(d for d in range(1, tp_size + 1) if tp_size % d == 0 and d * d <= tp_size)
    return tp_size // cols, cols


def flip(index, mask):
    bit = 1
    while bit <= mask:
        if mask & bit:
            index = index + bit * (1 - 2 * lax.rem(index // bit, 2))
        bit *= 2
    return index


def partner_order(sp_size):
    unit = sp_size // 8
    return unit, [k * unit + i for k in (2, 4, 3, 5, 6, 7, 0, 1) for i in range(unit)]


class Scatter:
    def __init__(self, grid, part, got, comb, got2, s1, r1, s2, r2):
        self.grid = grid
        self.part, self.got, self.comb, self.got2 = part, got, comb, got2
        self.s1, self.r1, self.s2, self.r2 = s1, r1, s2, r2

    def sizes(self, u):
        rows, cols = self.grid.shape
        return (cols, rows) if u % 2 == 0 else (rows, cols)

    def place(self, u, i, j):
        n1, n2 = self.sizes(u)
        return i * n2 + j if u % 2 == 0 else j * n2 + i

    def first(self, u, a):
        n1, n2 = self.sizes(u)
        peer = self.grid.along_row(a) if u % 2 == 0 else self.grid.along_col(a)
        span = pl.ds(a * n2, n2)
        return push(
            self.part.at[u, span], self.got.at[u, span], self.s1.at[u, a], self.r1.at[u, a], {"tp": peer}
        )

    def second(self, u, b):
        peer = self.grid.along_col(b) if u % 2 == 0 else self.grid.along_row(b)
        return push(self.comb.at[u, b], self.got2.at[u, b], self.s2.at[u, b], self.r2.at[u, b], {"tp": peer})

    def start(self, u):
        for a in range(1, self.sizes(u)[0]):
            self.first(u, a).start()

    def middle(self, u):
        n1, n2 = self.sizes(u)
        for a in range(1, n1):
            self.first(u, a).wait_recv()
        for b in range(1, n2):
            self.comb[u, b] = self.near_sum(u, b).astype(jnp.bfloat16)
            self.second(u, b).start()

    def near_sum(self, u, b):
        n1, n2 = self.sizes(u)
        acc = self.part[u, b].astype(jnp.float32)
        for a in range(1, n1):
            acc += self.got[u, a * n2 + b].astype(jnp.float32)
        return acc

    def finish(self, u):
        acc = self.near_sum(u, 0)
        for b in range(1, self.sizes(u)[1]):
            self.second(u, b).wait_recv()
            acc += self.got2[u, b].astype(jnp.float32)
        return acc

    def drain(self, u):
        n1, n2 = self.sizes(u)
        for a in range(1, n1):
            self.first(u, a).wait_send()
        for b in range(1, n2):
            self.second(u, b).wait_send()


class Grid:
    def __init__(self, tp_size):
        self.shape = grid_of(tp_size)
        me = lax.axis_index("tp")
        self.row, self.col = me // self.shape[1], lax.rem(me, self.shape[1])

    def at(self, i, j):
        rows, cols = self.shape
        return lax.rem(self.row + j, rows) * cols + lax.rem(self.col + i, cols)

    def along_row(self, i):
        return self.at(i, 0)

    def along_col(self, j):
        return self.at(0, j)

    def from_row(self, i):
        return self.at(self.shape[1] - i, 0)

    def from_col(self, j):
        return self.at(0, self.shape[0] - j)


def split_bf(x):
    high = x.astype(jnp.bfloat16)
    return high, (x - high.astype(jnp.float32)).astype(jnp.bfloat16)


def over_rows(a, b):
    return lax.dot_general(a, b, (((0,), (0,)), ((), ())), preferred_element_type=jnp.float32)


def over_lanes(a, b):
    return lax.dot_general(a, b, (((1,), (1,)), ((), ())), preferred_element_type=jnp.float32)


class Mixer:
    def __init__(self, heads, depth, sp_size, refs):
        (
            self.ask,
            self.keep,
            self.val,
            self.emit,
            self.key_v,
            self.cum_v,
            self.read_v,
            self.gate_v,
            self.qx_v,
            self.own,
            self.par,
            self.chip_own,
            self.chip_in,
            self.carry_f,
            self.carry_own,
            self.carry_par,
            self.mixed,
            self.pair_send,
            self.pair_recv,
            self.chip_send,
            self.chip_recv,
            self.carry_send,
            self.carry_recv,
        ) = refs
        self.heads, self.depth = heads, depth
        self.half = depth // 2
        self.body = heads * self.half
        self.chips = sp_size // 2
        self.me = lax.axis_index("sp")
        self.core = lax.rem(self.me, 2)
        self.chip = self.me // 2
        self.partner = self.me + 1 - 2 * self.core
        self.tokens = self.ask.shape[0]
        self.chunk = self.tokens // 2

    def lanes_of(self, h):
        return slice(h * self.depth, (h + 1) * self.depth)

    def rows_of(self, c):
        return slice(c * self.chunk, (c + 1) * self.chunk)

    def pair_copy(self):
        return push(self.own, self.par, self.pair_send, self.pair_recv, {"sp": self.partner})

    def chip_copy(self, d):
        return push(
            self.chip_own, self.chip_in.at[d], self.chip_send.at[d], self.chip_recv.at[d], {"sp": self.me + 2 * d}
        )

    def carry_copy(self):
        return push(self.carry_own, self.carry_par, self.carry_send, self.carry_recv, {"sp": self.partner})

    def states(self, share_ref, tok):
        f32, bf = jnp.float32, jnp.bfloat16
        n = self.chunk
        lower = lax.broadcasted_iota(jnp.int32, (n, n), 1) <= lax.broadcasted_iota(jnp.int32, (n, n), 0)
        lower = lower.astype(f32).astype(bf)
        for h in range(self.heads):
            lanes = self.lanes_of(h)
            share = share_ref[:, lanes]
            kept = share + (1.0 - share) * jax.nn.sigmoid(self.keep[:, lanes].astype(f32))
            key = 1.0 - kept
            decay = jnp.log(kept) + tok[:, 5 + h : 6 + h]
            self.key_v[:, lanes] = key
            parts, ends = [], []
            for c in range(2):
                rows = self.rows_of(c)
                d1, d2 = split_bf(decay[rows])
                d3 = (decay[rows] - d1.astype(f32) - d2.astype(f32)).astype(bf)
                sums = jnp.dot(lower, jnp.concatenate([d1, d2, d3], axis=1), preferred_element_type=f32)
                w = self.depth
                cum = sums[:, :w] + sums[:, w : 2 * w] + sums[:, 2 * w :]
                self.cum_v[rows, lanes] = cum
                end = cum[n - 1 : n]
                ends.append(end)
                late = jnp.concatenate(split_bf(key[rows] * jnp.exp(end - cum)), axis=1)
                state = over_rows(self.val[rows, lanes], late)
                parts.append(state[:, :w] + state[:, w:])
            self.read_v[self.rows_of(1), lanes] = parts[0]
            state = (parts[0] * jnp.exp(ends[1]) + parts[1]).astype(bf)
            total = jnp.exp(ends[0] + ends[1]).astype(bf)
            for k in range(2):
                self.own[k, h * self.half : (h + 1) * self.half] = state[k * self.half : (k + 1) * self.half]
                self.own[k, self.body + h : self.body + h + 1] = total

    def total_of(self, ref, h):
        return ref[self.body + h : self.body + h + 1].astype(jnp.float32)

    def join(self):
        f32, bf = jnp.float32, jnp.bfloat16
        self.pair_copy().wait_recv()
        own, par = self.own.at[self.core], self.par.at[self.core]
        odd = self.core == 1
        for h in range(self.heads):
            rows = slice(h * self.half, (h + 1) * self.half)
            mine, other = own[rows].astype(f32), par[rows].astype(f32)
            mine_t, other_t = self.total_of(own, h), self.total_of(par, h)
            joined = jnp.where(odd, other * mine_t + mine, mine * other_t + other)
            self.chip_own[rows] = joined.astype(bf)
            self.chip_own[self.body + h : self.body + h + 1] = (mine_t * other_t).astype(bf)
        for d in reversed(range(1, self.chips)):

            @pl.when(self.chip + d < self.chips)
            def _(d=d):
                self.chip_copy(d).start()

    def inside(self, gain_ref):
        f32, bf = jnp.float32, jnp.bfloat16
        n = self.chunk
        causal = lax.broadcasted_iota(jnp.int32, (n, n), 1) <= lax.broadcasted_iota(jnp.int32, (n, n), 0)
        for h in range(self.heads):
            lanes = self.lanes_of(h)
            first_end = None
            for c in range(2):
                rows = self.rows_of(c)
                raw = self.ask[rows, lanes].astype(f32)
                query = raw * jax.nn.sigmoid(raw)
                cum, key = self.cum_v[rows, lanes], self.key_v[rows, lanes]
                middle = cum[n // 2 - 1 : n // 2]
                q_mid = query * jnp.exp(cum - middle)
                q1, q2 = split_bf(q_mid)
                k1, k2 = split_bf(key * jnp.exp(middle - cum))
                scores = over_lanes(
                    jnp.concatenate([q1, q2, q1], axis=1), jnp.concatenate([k1, k1, k2], axis=1)
                )
                scores = jnp.where(causal, scores, 0.0)
                values = self.val[rows, lanes]
                read = jnp.dot(
                    jnp.concatenate(split_bf(scores), axis=1),
                    jnp.concatenate([values, values], axis=0),
                    preferred_element_type=f32,
                )
                q_start = query * jnp.exp(cum)
                if c == 0:
                    first_end = cum[n - 1 : n]
                else:
                    early = self.read_v[rows, lanes]
                    q_pair = jnp.concatenate(split_bf(q_start), axis=1)
                    e1 = early.astype(bf)
                    read += over_lanes(q_pair, jnp.concatenate([e1, e1], axis=1))
                    q_start = q_start * jnp.exp(first_end)
                self.read_v[rows, lanes] = read
                w = self.depth
                self.qx_v[rows, 2 * h * w : 2 * (h + 1) * w] = jnp.concatenate(split_bf(q_start), axis=1)
                raw = self.emit[rows, lanes].astype(f32)
                self.gate_v[rows, lanes] = raw * jax.nn.sigmoid(raw) * gain_ref[...]

    def carry(self):
        f32, bf = jnp.float32, jnp.bfloat16
        self.carry_f[...] = jnp.zeros_like(self.carry_f)
        shape = (1, self.depth)
        factors = [jnp.ones(shape, f32) for _ in range(self.heads)]
        for d in range(1, self.chips):
            there = self.chip >= d

            @pl.when(there)
            def _(d=d):
                self.chip_copy(d).wait_recv()
                for h in range(self.heads):
                    rows = slice(h * self.half, (h + 1) * self.half)
                    scale = jnp.ones(shape, f32)
                    for e in range(1, d):
                        scale = scale * self.total_of(self.chip_in.at[e], h)
                    self.carry_f[rows] += scale * self.chip_in[d, rows].astype(f32)

        self.carry_own[...] = self.carry_f[...].astype(bf)
        self.carry_copy().start()

    def outside(self):
        f32, bf = jnp.float32, jnp.bfloat16
        self.carry_copy().wait_recv()
        odd = self.core == 1
        for h in range(self.heads):
            lanes = self.lanes_of(h)
            rows = slice(h * self.half, (h + 1) * self.half)
            mine, other = self.carry_own[rows].astype(f32), self.carry_par[rows].astype(f32)
            low, high = jnp.where(odd, other, mine), jnp.where(odd, mine, other)
            start = jnp.concatenate([low, high], axis=0)
            before = jnp.concatenate([self.par[0, rows], self.par[1, rows]], axis=0).astype(f32)
            later = start * self.total_of(self.par.at[0], h) + before
            state = jnp.where(odd, later, start).astype(bf)
            w = self.depth
            read = self.read_v[:, lanes] + over_lanes(
                self.qx_v[:, 2 * h * w : 2 * (h + 1) * w], jnp.concatenate([state, state], axis=1)
            )
            level = jnp.mean(read * read, axis=1, keepdims=True)
            self.mixed[:, lanes] = (read * lax.rsqrt(level + EPS) * self.gate_v[:, lanes]).astype(bf)

    def drain(self):
        self.pair_copy().wait_send()
        self.carry_copy().wait_send()
        for d in range(1, self.chips):

            @pl.when(self.chip + d < self.chips)
            def _(d=d):
                self.chip_copy(d).wait_send()


def layer_kernel(
    sp_size,
    tp_size,
    cap,
    heads,
    depth,
    ids_ref,
    chance_ref,
    duo_ref,
    shrink_ref,
    gain_ref,
    share_ref,
    lane_gain_ref,
    ask_hbm,
    keep_hbm,
    val_hbm,
    emit_hbm,
    skip_hbm,
    proj_hbm,
    gate_hbm,
    up_hbm,
    down_hbm,
    out_ref,
    resid_v,
    *scratch,
):
    mixer_refs, scratch = scratch[:23], scratch[23:]
    (
    gate_w,
    up_w,
    down_w,
    proj_w,
    skip_v,
    pj_part,
    pj_got,
    pj_comb,
    pj_got2,
    tok_v,
    sq,
    scale_out,
    scale_in,
    scale_v,
    oh0,
    oh1,
    slots_in,
    arr,
    part,
    got,
    comb,
    got2,
    hid,
    slots,
    ret,
    load_sem,
    pj_s1,
    pj_r1,
    pj_s2,
    pj_r2,
    sq_send,
    sq_recv,
    scale_send,
    scale_recv,
    out_send,
    out_recv,
    own_row_send,
    own_row_recv,
    own_col_send,
    own_col_recv,
    relay_send,
    relay_recv,
    rs_s1,
    rs_r1,
    rs_s2,
    rs_r2,
    back_send,
    back_recv,
    ) = scratch
    my_s = lax.axis_index("sp")
    my_t = lax.axis_index("tp")
    grid = Grid(tp_size)
    grid_rows, grid_cols = grid.shape
    unit, masks = partner_order(sp_size)
    units = sp_size // unit
    unit_rows = unit * cap
    tokens, width = out_ref.shape
    model_width, hidden_width = gate_w.shape
    bf, f32 = jnp.bfloat16, jnp.float32
    pj_units, pj_rows = pj_part.shape[0], pj_part.shape[2]

    mix = Mixer(heads, depth, sp_size, mixer_refs)
    my_cols = pl.ds(pl.multiple_of(my_t * width, width), width)
    pairs_in = (
        (keep_hbm, mix.keep),
        (val_hbm, mix.val),
        (ask_hbm, mix.ask),
        (emit_hbm, mix.emit),
        (proj_hbm, proj_w),
        (skip_hbm.at[:, my_cols], skip_v),
        (gate_hbm, gate_w),
        (up_hbm, up_w),
        (down_hbm, down_w),
    )
    loads = [pltpu.make_async_copy(src, dst, load_sem.at[i]) for i, (src, dst) in enumerate(pairs_in)]
    barrier = pltpu.get_barrier_semaphore()

    def tp_of(j):
        return lax.rem(my_t + j, tp_size)

    def sp_of(q):
        return flip(my_s, masks[q])

    others = [q for q in range(sp_size) if masks[q]]
    home = masks.index(0)

    each(
        1,
        tp_size,
        lambda j: pl.semaphore_signal(barrier, inc=1, device_id={"tp": tp_of(j)}, device_id_type=MESH),
    )
    for q in others:
        pl.semaphore_signal(barrier, inc=1, device_id={"sp": sp_of(q)}, device_id_type=MESH)
    for load in loads:
        load.start()
    tok_v[...] = jnp.zeros_like(tok_v)
    tok_v[0:2] = ids_ref[...].astype(f32)
    tok_v[2:3] = chance_ref[...]
    tok_v[3:5] = duo_ref[...]
    tok_v[5 : 5 + heads] = shrink_ref[...]
    tok = jnp.transpose(tok_v[...])
    with jax.named_scope("states"):
        loads[0].wait()
        loads[1].wait()
        mix.states(share_ref, tok)
    with jax.named_scope("barrier"):
        pl.semaphore_wait(barrier, tp_size + sp_size - 2)
    mix.pair_copy().start()
    lanes = -(-sp_size // 128) * 128
    lane = lax.broadcasted_iota(jnp.int32, (1, lanes), 1)
    base = jnp.zeros((1, lanes), f32)
    for q in range(sp_size):
        base = base + jnp.where(lane == sp_of(q), float(q * cap), 0.0)
    wide_lane = lax.broadcasted_iota(jnp.int32, (tokens, lanes), 1).astype(f32)
    mine = [(wide_lane == tok[:, j : j + 1]).astype(f32) for j in range(2)]
    row_id = lax.broadcasted_iota(jnp.int32, (tokens, tokens), 0)
    col_id = lax.broadcasted_iota(jnp.int32, (tokens, tokens), 1)
    before = (col_id < row_id).astype(f32).astype(bf)
    rank = jnp.dot(before, (mine[0] + mine[1]).astype(bf), preferred_element_type=f32) + base
    slot_ids = lax.broadcasted_iota(jnp.int32, (tokens, sp_size * cap), 1).astype(f32)
    for j, oh in enumerate((oh0, oh1)):
        spot = jnp.sum(rank * mine[j], axis=1, keepdims=True)
        oh[...] = (slot_ids == spot).astype(f32).astype(bf)
    weights = [
        tok[:, 2:3] * jax.nn.sigmoid(tok[:, 3:4] - tok[:, 4:5]),
        tok[:, 2:3] * jax.nn.sigmoid(tok[:, 4:5] - tok[:, 3:4]),
    ]

    with jax.named_scope("join"):
        mix.join()
        loads[2].wait()
        loads[3].wait()
    with jax.named_scope("inside"):
        mix.inside(lane_gain_ref)
    with jax.named_scope("carry"):
        mix.carry()
        loads[4].wait()
    with jax.named_scope("outside"):
        mix.outside()

    pj = Scatter(grid, pj_part, pj_got, pj_comb, pj_got2, pj_s1, pj_r1, pj_s2, pj_r2)

    def project(i, j):
        cols = pl.ds(pl.multiple_of(grid.at(i, j) * width, width), width)
        out = jnp.dot(mix.mixed[...], proj_w[:, cols], preferred_element_type=f32).astype(bf)
        for u in range(pj_units):
            pj_part[u, pj.place(u, i, j)] = out[u * pj_rows : (u + 1) * pj_rows]

    targets = [(i, j) for i in range(grid_cols) for j in range(grid_rows)]
    for i, j in targets:
        if i > 0:
            project(i, j)
    for i, j in targets:
        if i == 0 and j > 0:
            project(i, j)
    for u in range(pj_units):
        pj.start(u)
    project(0, 0)

    with jax.named_scope("pj_middle"):
        for u in range(pj_units):
            pj.middle(u)
        loads[5].wait()
    with jax.named_scope("pj_finish"):
        total = jnp.concatenate([pj.finish(u) for u in range(pj_units)], axis=0)
    resid = (skip_v[...].astype(f32) + total).astype(bf)
    resid_v[...] = resid
    wide = resid.astype(f32)
    scaled = (wide * gain_ref[:, my_cols]).astype(bf)

    both = oh0[...] + oh1[...]
    filled = lax.dot_general(
        both, scaled, (((0,), (0,)), ((), ())), preferred_element_type=f32
    ).astype(bf)
    slots_in[...] = filled.reshape(sp_size, cap, width)
    arr[my_t, home // unit, pl.ds((home % unit) * cap, cap)] = filled[home * cap : (home + 1) * cap]

    def out_copy(q):
        dst = arr.at[my_t, q // unit, pl.ds((q % unit) * cap, cap)]
        return push(slots_in.at[q], dst, out_send.at[q], out_recv.at[q], {"sp": sp_of(q)})

    def send_out(p):
        for q in range(p * unit, (p + 1) * unit):
            if q != home:
                out_copy(q).start()

    def sq_copy(j):
        return push(sq.at[0], sq.at[j], sq_send.at[j], sq_recv.at[j], {"tp": tp_of(j)})

    def scale_copy(q):
        return push(
            scale_out.at[q], scale_in.at[q], scale_send.at[q], scale_recv.at[q], {"sp": sp_of(q)}
        )

    def start_squares():
        row_sums = jnp.sum(wide * wide, axis=1, keepdims=True)
        sq[0] = jnp.transpose(jnp.broadcast_to(row_sums, (tokens, 128)))[:8]
        each(1, tp_size, lambda j: sq_copy(j).start())

    def send_scales():
        each(1, tp_size, lambda j: sq_copy(j).wait_recv())
        scale = lax.rsqrt(jnp.sum(sq[...], axis=0) / model_width + EPS)
        s1, s2 = split_bf(scale)
        s3 = (scale - s1.astype(f32) - s2.astype(f32)).astype(bf)
        picked = sum(jnp.dot(term, both, preferred_element_type=f32) for term in (s1, s2, s3))
        for q in range(sp_size):
            dst = scale_in if q == home else scale_out
            dst[q, :, 0:cap] = picked[:, q * cap : (q + 1) * cap]
        for q in others:
            scale_copy(q).start()

    def column_of(g):
        cols = []
        for q in range(2 * g * unit, 2 * (g + 1) * unit):
            if q != home:
                scale_copy(q).wait_recv()
            tall = jnp.transpose(jnp.broadcast_to(scale_in[q, 0:1], (128, 128)))
            cols.append(tall[:cap])
        scale_v[...] = jnp.concatenate(cols, axis=0)

    def own_row(p, i):
        block = arr.at[my_t, p]
        return push(block, block, own_row_send.at[p, i], own_row_recv.at[p, i], {"tp": grid.along_row(i)})

    def own_col(p, j):
        block = arr.at[my_t, p]
        return push(block, block, own_col_send.at[p, j], own_col_recv.at[p, j], {"tp": grid.along_col(j)})

    def relay(p, i, j):
        if p % 2 == 0:
            block, peer = arr.at[grid.from_row(i), p], grid.along_col(j)
        else:
            block, peer = arr.at[grid.from_col(j), p], grid.along_row(i)
        return push(block, block, relay_send.at[p, i, j], relay_recv.at[p, i, j], {"tp": peer})

    def take(p):
        for i in range(unit):
            q = p * unit + i
            if q != home:
                out_copy(q).wait_recv()
        for i in range(1, grid_cols):
            own_row(p, i).start()
        for j in range(1, grid_rows):
            own_col(p, j).start()

    def pass_on(p):
        if p % 2 == 0:
            for i in range(1, grid_cols):
                own_row(p, i).wait_recv()
                for j in range(1, grid_rows):
                    relay(p, i, j).start()
        else:
            for j in range(1, grid_rows):
                own_col(p, j).wait_recv()
                for i in range(1, grid_cols):
                    relay(p, i, j).start()

    def gathered(p):
        if p % 2 == 0:
            for j in range(1, grid_rows):
                own_col(p, j).wait_recv()
        else:
            for i in range(1, grid_cols):
                own_row(p, i).wait_recv()
        for i in range(1, grid_cols):
            for j in range(1, grid_rows):
                relay(p, i, j).wait_recv()

    rs = Scatter(grid, part, got, comb, got2, rs_s1, rs_r1, rs_s2, rs_r2)
    tile = min(256, hidden_width)

    steps = hidden_width // tile

    def widen(g, first, last):
        pair = pl.ds(2 * g, 2)
        scale = scale_v[:, 0:1]

        @pl.loop(first, last)
        def _(f):
            cols = pl.ds(pl.multiple_of(f * tile, tile), tile)
            gate = jnp.zeros((2 * unit_rows, tile), f32)
            up = jnp.zeros((2 * unit_rows, tile), f32)
            for t in range(tp_size):
                depth = slice(t * width, (t + 1) * width)
                x = arr[t, pair].reshape(2 * unit_rows, width)
                gate += jnp.dot(x, gate_w[depth, cols], preferred_element_type=f32)
                up += jnp.dot(x, up_w[depth, cols], preferred_element_type=f32)
            gate, up = gate * scale, up * scale
            hid[:, cols] = (gate * jax.nn.sigmoid(gate) * up).astype(bf)

    def narrow(g):
        def lower(i, j):
            cols = pl.ds(pl.multiple_of(grid.at(i, j) * width, width), width)
            out = jnp.dot(hid[...], down_w[:, cols], preferred_element_type=f32).astype(bf)
            part[2 * g, rs.place(2 * g, i, j)] = out[:unit_rows]
            part[2 * g + 1, rs.place(2 * g + 1, i, j)] = out[unit_rows:]

        for i in range(1, grid_cols):
            for j in range(grid_rows):
                lower(i, j)
        rs.start(2 * g)
        for j in range(1, grid_rows):
            lower(0, j)
        rs.start(2 * g + 1)
        lower(0, 0)

    def back_copy(q):
        return push(slots.at[q], ret.at[q], back_send.at[q], back_recv.at[q], {"sp": sp_of(q)})

    def give_back(p):
        done = rs.finish(p).astype(bf)
        for i in range(unit):
            q = p * unit + i
            if q == home:
                ret[home] = done[i * cap : (i + 1) * cap]
            else:
                slots[q] = done[i * cap : (i + 1) * cap]
                back_copy(q).start()

    def stage(name, *calls):
        with jax.named_scope(name):
            for call, p in calls:
                call(p)

    def both_of(call, g):
        return (call, 2 * g), (call, 2 * g + 1)

    def expert(g, *between):
        stage(f"gathered_{g}", *both_of(gathered, g))
        with jax.named_scope(f"widen_{g}"):
            column_of(g)
            widen(g, 0, steps // 2)
        stage(f"serve_{g}", *between)
        with jax.named_scope(f"narrow_{g}"):
            widen(g, steps // 2, steps)
            narrow(g)

    for p in (7, 0, 1):
        send_out(p)
    take(6)
    with jax.named_scope("squares"):
        start_squares()
    stage("take_1", (take, 7))
    with jax.named_scope("scales"):
        send_scales()
    stage("pass_a", (pass_on, 6), (send_out, 3), (pass_on, 7))
    stage("take_b", (take, 0), (send_out, 4), (take, 1), (send_out, 5), (send_out, 2))
    stage("pass_b", (pass_on, 0), (take, 3), (pass_on, 1), (take, 2))
    for load in loads[6:]:
        load.wait()
    expert(0, (pass_on, 2), (pass_on, 3))
    stage("take_c", (take, 4))
    expert(1, (take, 5), (pass_on, 4), *both_of(rs.middle, 0))
    stage("take_d", (pass_on, 5), *both_of(give_back, 0))
    expert(2, *both_of(rs.middle, 1))
    stage("back_1", *both_of(give_back, 1))
    expert(3)
    stage("middle_2", *both_of(rs.middle, 2))
    stage("back_2", *both_of(give_back, 2))
    stage("middle_3", *both_of(rs.middle, 3))
    stage("back_3", *both_of(give_back, 3))

    with jax.named_scope("back_wait"):
        for q in others:
            back_copy(q).wait_recv()
    returned = ret[...].reshape(sp_size * cap, width)
    mixed = jnp.zeros((tokens, width), f32)
    for j, oh in enumerate((oh0, oh1)):
        mixed += weights[j] * jnp.dot(oh[...], returned, preferred_element_type=f32)
    out_ref[...] = mixed

    mix.drain()
    for u in range(pj_units):
        pj.drain(u)
    for p in range(units):
        for i in range(1, grid_cols):
            own_row(p, i).wait_send()
            for j in range(1, grid_rows):
                relay(p, i, j).wait_send()
        for j in range(1, grid_rows):
            own_col(p, j).wait_send()
        rs.drain(p)
    each(1, tp_size, lambda j: sq_copy(j).wait_send())
    for q in others:
        scale_copy(q).wait_send()
        out_copy(q).wait_send()
        back_copy(q).wait_send()


def run_layer(
    ids, chance, duo, shrink, gain, share, lane_gain, ask, keep, val, emit, skip, projection, gate, up, down, cap, heads
):
    sp_size = lax.axis_size("sp")
    tp_size = lax.axis_size("tp")
    grid_rows, grid_cols = grid_of(tp_size)
    side = max(grid_rows, grid_cols)
    tokens, model_width = skip.shape
    width = model_width // tp_size
    hidden_width = gate.shape[1]
    unit, masks = partner_order(sp_size)
    units = sp_size // unit
    rows = unit * cap
    quarter = tokens // 4
    depth = lane_gain.shape[1]
    chips = sp_size // 2
    mixer_width = heads * depth
    body = heads * depth // 2
    packed = body + heads + (-heads) % 16
    bf, f32 = jnp.bfloat16, jnp.float32
    dma = pltpu.SemaphoreType.DMA
    anywhere = pl.BlockSpec(memory_space=pl.ANY)
    vmem = pltpu.VMEM
    return pl.pallas_call(
        functools.partial(layer_kernel, sp_size, tp_size, cap, heads, depth),
        out_shape=(
            jax.ShapeDtypeStruct((tokens, width), f32),
            jax.ShapeDtypeStruct((tokens, width), bf),
        ),
        in_specs=[VMEM] * 7 + [anywhere] * 9,
        out_specs=(VMEM, VMEM),
        scratch_shapes=[
            vmem((tokens, mixer_width), bf),
            vmem((tokens, mixer_width), bf),
            vmem((tokens, mixer_width), bf),
            vmem((tokens, mixer_width), bf),
            vmem((tokens, mixer_width), f32),
            vmem((tokens, mixer_width), f32),
            vmem((tokens, mixer_width), f32),
            vmem((tokens, mixer_width), f32),
            vmem((tokens, 2 * mixer_width), bf),
            vmem((2, packed, depth), bf),
            vmem((2, packed, depth), bf),
            vmem((packed, depth), bf),
            vmem((chips, packed, depth), bf),
            vmem((body, depth), f32),
            vmem((body, depth), bf),
            vmem((body, depth), bf),
            vmem((tokens, mixer_width), bf),
            dma(()),
            dma(()),
            dma((chips,)),
            dma((chips,)),
            dma(()),
            dma(()),
            vmem(gate.shape, bf),
            vmem(up.shape, bf),
            vmem(down.shape, bf),
            vmem(projection.shape, bf),
            vmem((tokens, width), bf),
            vmem((4, tp_size, quarter, width), bf),
            vmem((4, tp_size, quarter, width), bf),
            vmem((4, side, quarter, width), bf),
            vmem((4, side, quarter, width), bf),
            vmem((128, tokens), f32),
            vmem((tp_size, 8, tokens), f32),
            vmem((sp_size, 8, 128), f32),
            vmem((sp_size, 8, 128), f32),
            vmem((2 * rows, 128), f32),
            vmem((tokens, sp_size * cap), bf),
            vmem((tokens, sp_size * cap), bf),
            vmem((sp_size, cap, width), bf),
            vmem((tp_size, units, rows, width), bf),
            vmem((units, tp_size, rows, width), bf),
            vmem((units, tp_size, rows, width), bf),
            vmem((units, side, rows, width), bf),
            vmem((units, side, rows, width), bf),
            vmem((2 * rows, hidden_width), bf),
            vmem((sp_size, cap, width), bf),
            vmem((sp_size, cap, width), bf),
            dma((9,)),
            dma((4, side)),
            dma((4, side)),
            dma((4, side)),
            dma((4, side)),
            dma((tp_size,)),
            dma((tp_size,)),
            dma((sp_size,)),
            dma((sp_size,)),
            dma((sp_size,)),
            dma((sp_size,)),
            dma((units, grid_cols)),
            dma((units, grid_cols)),
            dma((units, grid_rows)),
            dma((units, grid_rows)),
            dma((units, grid_cols, grid_rows)),
            dma((units, grid_cols, grid_rows)),
            dma((units, side)),
            dma((units, side)),
            dma((units, side)),
            dma((units, side)),
            dma((sp_size,)),
            dma((sp_size,)),
        ],
        compiler_params=pltpu.CompilerParams(
            collective_id=1, has_side_effects=True, vmem_limit_bytes=VMEM_LIMIT
        ),
    )(ids, chance, duo, shrink, gain, share, lane_gain, ask, keep, val, emit, skip, projection, gate, up, down)


def shards(
    skip_path_vectors,
    asker_raw_scores,
    retain_raw_scores,
    memory_write_entries,
    emit_switch_scores,
    retain_minimum_share,
    extra_shrink_rate,
    lane_rescale_factor,
    emit_projection_array,
    specialist_rescale_factor,
    specialist_switch_proj,
    specialist_raise_proj,
    specialist_lower_proj,
    specialist_choice_ids,
    cluster_chance,
    specialist_duo_scores,
):
    tokens = skip_path_vectors.shape[0]
    heads = extra_shrink_rate.shape[0]
    experts = lax.axis_size("sp")
    top_count = specialist_choice_ids.shape[1]
    capacity = -(-3 * tokens * top_count // (2 * experts))
    capacity = -(-capacity // 16) * 16
    routed, resid = run_layer(
        specialist_choice_ids.T,
        cluster_chance[None, :],
        specialist_duo_scores.T,
        extra_shrink_rate,
        specialist_rescale_factor[None, :],
        retain_minimum_share[None, :],
        lane_rescale_factor[None, :],
        asker_raw_scores,
        retain_raw_scores,
        memory_write_entries,
        emit_switch_scores,
        skip_path_vectors,
        emit_projection_array,
        specialist_switch_proj[0],
        specialist_raise_proj[0],
        specialist_lower_proj[0],
        capacity,
        heads,
    )
    return (resid.astype(jnp.float32) + routed).astype(jnp.bfloat16)


def solution(mesh):
    return jax.shard_map(
        shards,
        mesh=mesh,
        in_specs=(
            P("sp", None),
            P("sp", "tp"),
            P("sp", "tp"),
            P("sp", "tp"),
            P("sp", "tp"),
            P("tp"),
            P("tp", "sp"),
            P(),
            P("tp", None),
            P(),
            P("sp", None, "tp"),
            P("sp", None, "tp"),
            P("sp", "tp", None),
            P("sp", None),
            P("sp"),
            P("sp", None),
        ),
        out_specs=P("sp", "tp"),
        check_vma=False,
    )
```

time: 128 us -> 100 us (0.78); the launches traced: 127 us -> 100 us
  Pallas kernels: 108 us -> 98.3 us
  local copies, waits for them, and re-layouts: 7.87 us -> 0 us
  other arithmetic: 6.62 us -> 1.88 us
  matrix products: 3.91 us -> 0 us
    pallas_call x2 -> x1, Pallas kernels: 108 us -> 98.3 us  [run_layer(): pl.pallas_call(functools.partial(layer_kernel, sp_size, tp_size, cap, hea...]
    dot_general x4 -> x0, matrix products: 3.91 us -> none  [the longest x1 1.49 us: shards(): jnp.einsum('thd,hdv->thv', query_tilde, carried, precision=PRECISE)]
    unnamed x17 -> x0, local copies, waits for them, and re-layouts: 3 us -> none
    convert_element_type x8 -> x0, local copies, waits for them, and re-layouts: 1.64 us -> none  [the longest x1 0.84 us: shards(): gated_out.reshape(token_count_total, lanes_on_device * head_depth)]
    sub x2 -> x0, other arithmetic: 1.58 us -> none  [the longest x1 0.9 us: shards(): key_rows = 1.0 - retain_share]
    select_n x2 -> x0, other arithmetic: 1.51 us -> none  [the longest x1 0.92 us: carry_states(): carried = carried + jnp.where(earlier, held, 0.0)]
    slice x1 -> x0, local copies, waits for them, and re-layouts: 1.31 us -> none  [carry_states(): held = states[lap].astype(jnp.float32) * factor[:, :, None]]
where the time goes in v2:
time: 100 us
  Pallas kernels  98.3 us (98%)
  other arithmetic  1.88 us (2%)
    pallas_call x1, Pallas kernels, run_layer(): pl.pallas_call(functools.partial(layer_kernel, sp_size, tp_size, cap, hea...  98.3 us

profile of v2, /device:TPU:1, one launch (start us, length us, event | category | flops | bytes accessed | tf_op | source)
XLA Modules:
  0.0 100.2 jit_solution(14213534769800298794)
XLA Ops:
  0.0 98.3 %shard_map.154 = (f32[256,512]{1,0:T(8,128)}, bf16[256,512]{1,0:T(8,128)(2,1)}) custom-call(s32[2,256]{1,0:T(2,128)} %bitcast.13, f32[1,256]{1,0:T(1,128)} %bitcast.16, f32[2,256]{1,0:T(2,128)} %bitcast.14, f32[4,256]{1,0:T(4,128)} %shrink_ref.1, f32[1,2048]{1,0:T(1,128)} %bitcast.12, f32[1,512]{1,0:T(1,128)} %bitcast.15, f32[1,128]{1,0:T(1,128)} %bitcast.17, ...), custom_call_target="tpu_custom_call" | custom-call | tf_op jit(solution)/shard_map/pallas_call | solution.py:794
  98.3 1.9 %add_convert_fusion = bf16[256,512]{1,0:T(8,128)(2,1)} fusion(f32[256,512]{1,0:T(8,128)} %get-tuple-element.8, bf16[256,512]{1,0:T(8,128)(2,1)} %get-tuple-element.7), kind=kLoop, calls=%fused_computation | loop fusion | flops 393216 | bytes 1048576 | tf_op jit(solution)/shard_map/convert_element_type | solution.py:925

commit v3 on v2

--- a/solution.py
+++ b/solution.py
@@ -73,12 +73,12 @@
         peer = self.grid.along_row(a) if u % 2 == 0 else self.grid.along_col(a)
         span = pl.ds(a * n2, n2)
         return push(
-            self.part.at[u, span], self.got.at[u, span], self.s1.at[u, a], self.r1.at[u, a], {"tp": peer}
+            self.part.at[u, span], self.got.at[u, span], self.s1.at[u, a - 1], self.r1.at[u, a - 1], {"tp": peer}
         )
 
     def second(self, u, b):
         peer = self.grid.along_col(b) if u % 2 == 0 else self.grid.along_row(b)
-        return push(self.comb.at[u, b], self.got2.at[u, b], self.s2.at[u, b], self.r2.at[u, b], {"tp": peer})
+        return push(self.comb.at[u, b], self.got2.at[u, b], self.s2.at[u, b - 1], self.r2.at[u, b - 1], {"tp": peer})
 
     def start(self, u):
         for a in range(1, self.sizes(u)[0]):
@@ -199,7 +199,7 @@
 
     def chip_copy(self, d):
         return push(
-            self.chip_own, self.chip_in.at[d], self.chip_send.at[d], self.chip_recv.at[d], {"sp": self.me + 2 * d}
+            self.chip_own, self.chip_in.at[d], self.chip_send.at[d - 1], self.chip_recv.at[d - 1], {"sp": self.me + 2 * d}
         )
 
     def carry_copy(self):
@@ -373,8 +373,11 @@
     gate_hbm,
     up_hbm,
     down_hbm,
-    out_ref,
+    out_hbm,
+    mixed_v,
     resid_v,
+    result_v,
+    result_sem,
     *scratch,
 ):
     mixer_refs, scratch = scratch[:23], scratch[23:]
@@ -435,7 +438,7 @@
     unit, masks = partner_order(sp_size)
     units = sp_size // unit
     unit_rows = unit * cap
-    tokens, width = out_ref.shape
+    tokens, width = out_hbm.shape
     model_width, hidden_width = gate_w.shape
     bf, f32 = jnp.bfloat16, jnp.float32
     pj_units, pj_rows = pj_part.shape[0], pj_part.shape[2]
@@ -547,6 +550,12 @@
     resid = (skip_v[...].astype(f32) + total).astype(bf)
     resid_v[...] = resid
     wide = resid.astype(f32)
+    def sq_copy(j):
+        return push(sq.at[0], sq.at[j], sq_send.at[j - 1], sq_recv.at[j - 1], {"tp": tp_of(j)})
+
+    row_sums = jnp.sum(wide * wide, axis=1, keepdims=True)
+    sq[0] = jnp.transpose(jnp.broadcast_to(row_sums, (tokens, 128)))[:8]
+    each(1, tp_size, lambda j: sq_copy(j).start())
     scaled = (wide * gain_ref[:, my_cols]).astype(bf)
 
     both = oh0[...] + oh1[...]
@@ -565,18 +574,10 @@
             if q != home:
                 out_copy(q).start()
 
-    def sq_copy(j):
-        return push(sq.at[0], sq.at[j], sq_send.at[j], sq_recv.at[j], {"tp": tp_of(j)})
-
     def scale_copy(q):
         return push(
             scale_out.at[q], scale_in.at[q], scale_send.at[q], scale_recv.at[q], {"sp": sp_of(q)}
         )
-
-    def start_squares():
-        row_sums = jnp.sum(wide * wide, axis=1, keepdims=True)
-        sq[0] = jnp.transpose(jnp.broadcast_to(row_sums, (tokens, 128)))[:8]
-        each(1, tp_size, lambda j: sq_copy(j).start())
 
     def send_scales():
         each(1, tp_size, lambda j: sq_copy(j).wait_recv())
@@ -601,18 +602,18 @@
 
     def own_row(p, i):
         block = arr.at[my_t, p]
-        return push(block, block, own_row_send.at[p, i], own_row_recv.at[p, i], {"tp": grid.along_row(i)})
+        return push(block, block, own_row_send.at[p, i - 1], own_row_recv.at[p, i - 1], {"tp": grid.along_row(i)})
 
     def own_col(p, j):
         block = arr.at[my_t, p]
-        return push(block, block, own_col_send.at[p, j], own_col_recv.at[p, j], {"tp": grid.along_col(j)})
+        return push(block, block, own_col_send.at[p, j - 1], own_col_recv.at[p, j - 1], {"tp": grid.along_col(j)})
 
     def relay(p, i, j):
         if p % 2 == 0:
             block, peer = arr.at[grid.from_row(i), p], grid.along_col(j)
         else:
             block, peer = arr.at[grid.from_col(j), p], grid.along_row(i)
-        return push(block, block, relay_send.at[p, i, j], relay_recv.at[p, i, j], {"tp": peer})
+        return push(block, block, relay_send.at[p, i - 1, j - 1], relay_recv.at[p, i - 1, j - 1], {"tp": peer})
 
     def take(p):
         for i in range(unit):
@@ -716,15 +717,26 @@
             widen(g, steps // 2, steps)
             narrow(g)
 
+    def combine(first, last):
+        for q in range(first, last):
+            if q != home:
+                back_copy(q).wait_recv()
+        span = slice(first * cap, last * cap)
+        returned = ret[first:last].reshape((last - first) * cap, width)
+        mixed = mixed_v[...] if first else resid_v[...].astype(f32)
+        for j, oh in enumerate((oh0, oh1)):
+            mixed += weights[j] * jnp.dot(oh[:, span], returned, preferred_element_type=f32)
+        if last < sp_size:
+            mixed_v[...] = mixed
+        else:
+            result_v[...] = mixed.astype(bf)
+
     for p in (7, 0, 1):
         send_out(p)
-    take(6)
-    with jax.named_scope("squares"):
-        start_squares()
-    stage("take_1", (take, 7))
+    stage("take_a", (take, 6), (take, 7))
+    stage("pass_a", (pass_on, 6), (send_out, 3), (pass_on, 7))
     with jax.named_scope("scales"):
         send_scales()
-    stage("pass_a", (pass_on, 6), (send_out, 3), (pass_on, 7))
     stage("take_b", (take, 0), (send_out, 4), (take, 1), (send_out, 5), (send_out, 2))
     stage("pass_b", (pass_on, 0), (take, 3), (pass_on, 1), (take, 2))
     for load in loads[6:]:
@@ -737,35 +749,37 @@
     stage("back_1", *both_of(give_back, 1))
     expert(3)
     stage("middle_2", *both_of(rs.middle, 2))
+    with jax.named_scope("combine_a"):
+        combine(0, 2 * unit)
     stage("back_2", *both_of(give_back, 2))
     stage("middle_3", *both_of(rs.middle, 3))
+    with jax.named_scope("combine_b"):
+        combine(2 * unit, 4 * unit)
     stage("back_3", *both_of(give_back, 3))
-
-    with jax.named_scope("back_wait"):
+    with jax.named_scope("combine_c"):
+        combine(4 * unit, 8 * unit)
+
+    result_copy = pltpu.make_async_copy(result_v, out_hbm, result_sem)
+    result_copy.start()
+    with jax.named_scope("drain"):
+        mix.drain()
+        for u in range(pj_units):
+            pj.drain(u)
+        for p in range(units):
+            for i in range(1, grid_cols):
+                own_row(p, i).wait_send()
+                for j in range(1, grid_rows):
+                    relay(p, i, j).wait_send()
+            for j in range(1, grid_rows):
+                own_col(p, j).wait_send()
+            rs.drain(p)
+        each(1, tp_size, lambda j: sq_copy(j).wait_send())
         for q in others:
-            back_copy(q).wait_recv()
-    returned = ret[...].reshape(sp_size * cap, width)
-    mixed = jnp.zeros((tokens, width), f32)
-    for j, oh in enumerate((oh0, oh1)):
-        mixed += weights[j] * jnp.dot(oh[...], returned, preferred_element_type=f32)
-    out_ref[...] = mixed
-
-    mix.drain()
-    for u in range(pj_units):
-        pj.drain(u)
-    for p in range(units):
-        for i in range(1, grid_cols):
-            own_row(p, i).wait_send()
-            for j in range(1, grid_rows):
-                relay(p, i, j).wait_send()
-        for j in range(1, grid_rows):
-            own_col(p, j).wait_send()
-        rs.drain(p)
-    each(1, tp_size, lambda j: sq_copy(j).wait_send())
-    for q in others:
-        scale_copy(q).wait_send()
-        out_copy(q).wait_send()
-        back_copy(q).wait_send()
+            scale_copy(q).wait_send()
+            out_copy(q).wait_send()
+            back_copy(q).wait_send()
+    with jax.named_scope("result"):
+        result_copy.wait()
 
 
 def run_layer(
@@ -793,13 +807,14 @@
     vmem = pltpu.VMEM
     return pl.pallas_call(
         functools.partial(layer_kernel, sp_size, tp_size, cap, heads, depth),
-        out_shape=(
-            jax.ShapeDtypeStruct((tokens, width), f32),
-            jax.ShapeDtypeStruct((tokens, width), bf),
-        ),
+        out_shape=jax.ShapeDtypeStruct((tokens, width), bf),
         in_specs=[VMEM] * 7 + [anywhere] * 9,
-        out_specs=(VMEM, VMEM),
+        out_specs=anywhere,
         scratch_shapes=[
+            vmem((tokens, width), f32),
+            vmem((tokens, width), bf),
+            vmem((tokens, width), bf),
+            dma(()),
             vmem((tokens, mixer_width), bf),
             vmem((tokens, mixer_width), bf),
             vmem((tokens, mixer_width), bf),
@@ -819,8 +834,8 @@
             vmem((tokens, mixer_width), bf),
             dma(()),
             dma(()),
-            dma((chips,)),
-            dma((chips,)),
+            dma((chips - 1,)),
+            dma((chips - 1,)),
             dma(()),
             dma(()),
             vmem(gate.shape, bf),
@@ -849,26 +864,26 @@
             vmem((sp_size, cap, width), bf),
             vmem((sp_size, cap, width), bf),
             dma((9,)),
-            dma((4, side)),
-            dma((4, side)),
-            dma((4, side)),
-            dma((4, side)),
-            dma((tp_size,)),
-            dma((tp_size,)),
+            dma((4, side - 1)),
+            dma((4, side - 1)),
+            dma((4, side - 1)),
+            dma((4, side - 1)),
+            dma((tp_size - 1,)),
+            dma((tp_size - 1,)),
             dma((sp_size,)),
             dma((sp_size,)),
             dma((sp_size,)),
             dma((sp_size,)),
-            dma((units, grid_cols)),
-            dma((units, grid_cols)),
-            dma((units, grid_rows)),
-            dma((units, grid_rows)),
-            dma((units, grid_cols, grid_rows)),
-            dma((units, grid_cols, grid_rows)),
-            dma((units, side)),
-            dma((units, side)),
-            dma((units, side)),
-            dma((units, side)),
+            dma((units, grid_cols - 1)),
+            dma((units, grid_cols - 1)),
+            dma((units, grid_rows - 1)),
+            dma((units, grid_rows - 1)),
+            dma((units, grid_cols - 1, grid_rows - 1)),
+            dma((units, grid_cols - 1, grid_rows - 1)),
+            dma((units, side - 1)),
+            dma((units, side - 1)),
+            dma((units, side - 1)),
+            dma((units, side - 1)),
             dma((sp_size,)),
             dma((sp_size,)),
         ],
@@ -902,7 +917,7 @@
     top_count = specialist_choice_ids.shape[1]
     capacity = -(-3 * tokens * top_count // (2 * experts))
     capacity = -(-capacity // 16) * 16
-    routed, resid = run_layer(
+    return run_layer(
         specialist_choice_ids.T,
         cluster_chance[None, :],
         specialist_duo_scores.T,
@@ -922,7 +937,6 @@
         capacity,
         heads,
     )
-    return (resid.astype(jnp.float32) + routed).astype(jnp.bfloat16)
 
 
 def solution(mesh):

time: 100 us -> 99.7 us (level)
  other arithmetic: 1.88 us -> 0 us
  local copies, waits for them, and re-layouts: 0 us -> 1.67 us
    convert_element_type x1 -> x0, other arithmetic: 1.88 us -> none  [shards(): return (resid.astype(jnp.float32) + routed).astype(jnp.bfloat16)]
    unnamed x0 -> x1, local copies, waits for them, and re-layouts: none -> 1.67 us
where the time goes in v3:
time: 99.7 us; the launch traced here: 99.5 us
  Pallas kernels  97.9 us (98%)
  local copies, waits for them, and re-layouts  1.67 us (2%)
    pallas_call x1, Pallas kernels, run_layer(): pl.pallas_call(functools.partial(layer_kernel, sp_size, tp_size, cap, hea...  97.9 us

profile of v3, /device:TPU:1, one launch (start us, length us, event | category | flops | bytes accessed | tf_op | source)
XLA Modules:
  0.0 99.5 jit_solution(11582166121978727866)
XLA Ops:
  0.0 97.9 %shard_map.154 = bf16[256,512]{1,0:T(8,128)(2,1)} custom-call(s32[2,256]{1,0:T(2,128)} %bitcast.13, f32[1,256]{1,0:T(1,128)} %bitcast.16, f32[2,256]{1,0:T(2,128)} %bitcast.14, f32[4,256]{1,0:T(4,128)} %shrink_ref.1, f32[1,2048]{1,0:T(1,128)} %bitcast.12, f32[1,512]{1,0:T(1,128)} %bitcast.15, f32[1,128]{1,0:T(1,128)} %bitcast.17, bf16[256,512]{1,0:T(8,128)(2,1)} %ask_hbm.1, ...), custom_call_target="tpu_custom_call" | custom-call | tf_op jit(solution)/shard_map/pallas_call | solution.py:808
  97.9 1.7 %copy.18 = bf16[256,512]{1,0:T(8,128)(2,1)} copy(bf16[256,512]{1,0:T(8,128)(2,1)} %shard_map.154) | data formatting | bytes 524288
